TPU v7x, 256 devices: a 4x2x16 block of a 4x16x16 slice. The times are simulated.
256 devices in a mesh: grp: 2 (over y), sp: 32 (over z, core), tp: 4 (over x).
Axes of the slice: x: 4, y: 2, z: 16, core: 2. Of those that a mesh axis runs over, the one named last changes fastest.
The devices are a block of a 4x16x16 slice.
Arguments:
- receptance: bfloat16 [8192, 1024], P(('grp', 'sp'), 'tp'), parts along dimension 0, may hold values from -6 to 6
- head_keys: bfloat16 [8192, 1024], P(('grp', 'sp'), 'tp'), parts along dimension 0, may hold values from -6 to 6
- head_values: bfloat16 [8192, 1024], P(('grp', 'sp'), 'tp'), parts along dimension 0, may hold values from -6 to 6
- decay_logits: bfloat16 [8192, 1024], P(('grp', 'sp'), 'tp'), parts along dimension 0, may hold values from -13 to 0
- decay_boost: float32 [8192, 1024], P(('grp', 'sp'), 'tp'), parts along dimension 0, may hold values from -1.4 to 0
- correction_logits: bfloat16 [8192, 1024], P(('grp', 'sp'), 'tp'), parts along dimension 0, may hold values from -6 to 4
- gate_logits: bfloat16 [8192, 1024], P(('grp', 'sp'), 'tp'), parts along dimension 0, may hold values from -8 to 8
- head_norm_gain: float32 [1024], P('tp'), may hold values from 0.1 to 1.9
- output_weight: bfloat16 [1024, 2048], P('tp'), may hold values from -0.1875 to 0.1875
- residual: bfloat16 [8192, 2048], P(('grp', 'sp', 'tp')), parts along dimension 0, may hold values from -4 to 4
- expert_norm_gain: float32 [2048], replicated, may hold values from 0.1 to 1.9
- routes: int32 [8192, 2], P(('grp', 'sp', 'tp')), parts along dimension 0, may hold values from 0 to 31, all different within a row; in each aligned block of 32 rows (0 to 31, 32 to 63, ...) at most 4 rows name the same one
- routing_weight: float32 [8192, 2], P(('grp', 'sp', 'tp')), parts along dimension 0, may hold values from 0.1 to 1
- expert_gate_weight: bfloat16 [32, 2048, 3584], P('sp', None, 'tp'), may hold values from -0.125 to 0.125
- expert_up_weight: bfloat16 [32, 2048, 3584], P('sp', None, 'tp'), may hold values from -0.125 to 0.125
- expert_down_weight: bfloat16 [32, 3584, 2048], P('sp', 'tp'), may hold values from -0.09375 to 0.09375
Outputs:
- layer_out: bfloat16 [8192, 2048], P(('grp', 'sp', 'tp')), parts along dimension 0
There are 2 independent parts, one for each index of `grp`. A program takes and returns all parts, laid end to end along the dimension named above; an argument that names none is the same for every part. Nothing has to cross between parts.
Inputs may be any that keep to these rules, and one draw needn't show every extreme that they name: Each row names 2 different experts. Among the positions that one index of sp+tp holds in routes, no expert is named by more than 4 of them, and in every draw some expert is named by exactly 4 of them there.
All inputs are finite; a program needn't handle non-finite values.
Results may differ from a plain program's by a relative error of at most 0.017.
Values may be sent and summed in bfloat16 or wider, within the bound.
No kernel may reach another device: no remote copies, remote signals or barrier semaphores. Data moves between devices by JAX's collectives and lax.ppermute only.
A program may use at most 64 MiB of HBM per device.

v0:
```python
import math
from functools import partial

import jax
import jax.numpy as jnp
from jax import lax
from jax.experimental import pallas as pl
from jax.experimental.pallas import tpu as pltpu
from jax.sharding import Mesh
from jax.sharding import PartitionSpec as P


HEAD = 64
TOP = 2
BLK = 32
QUAD = 4
OFFSETS = (1, 3, 2)
FF_TILE = 256
LIMIT_FIRST = 42
LIMIT_REST = 18
HALF_DOWN = math.exp(-0.5)
TOK_DEV = 128
SP = ("sp_0", "sp_1")
GRP_SP = ("grp", "sp_0", "sp_1")
GRP_SP_TP = ("grp", "sp_0", "sp_1", "tp")


highest = lax.Precision.HIGHEST


def shifted(x, axis, step):
    size = lax.axis_size(axis)
    return lax.ppermute(x, axis, [(i, (i + step) % size) for i in range(size)])


def within_quads(x, axis, step):
    size = lax.axis_size(axis)
    pairs = [(i, i // QUAD * QUAD + (i % QUAD + step) % QUAD) for i in range(size)]
    return lax.ppermute(x, axis, pairs)


def across_quads(x, axis, step):
    size = lax.axis_size(axis)
    return lax.ppermute(x, axis, [(i, i + step * QUAD) for i in range(size - step * QUAD)])


def after(later, earlier):
    moved = jnp.einsum("hij,hjk->hik", later[..., :HEAD], earlier, precision=highest)
    return moved + jnp.where(jnp.arange(2 * HEAD) < HEAD, 0.0, later)


def onto(later, state):
    moved = jnp.einsum("hij,hjk->hik", later[..., :HEAD], state, precision=highest)
    return moved + later[..., HEAD:]


def incoming_state(packed):
    wide = jnp.float32
    core = lax.axis_index("sp_1")
    own = packed.astype(wide)
    other = shifted(packed, "sp_1", 1).astype(wide)
    first = jnp.where(core == 0, own, other)
    second = jnp.where(core == 0, other, own)
    half = own.shape[0] // 2
    chip = after(
        lax.dynamic_slice_in_dim(second, core * half, half, 0),
        lax.dynamic_slice_in_dim(first, core * half, half, 0),
    )
    sent = chip.astype(jnp.bfloat16)
    member = lax.axis_index("sp_0") % QUAD
    came = [chip] + [within_quads(sent, "sp_0", k).astype(wide) for k in range(1, QUAD)]
    came = jnp.stack(came)
    total = lax.dynamic_index_in_dim(came, member % QUAD, 0, False)
    eye = jnp.eye(HEAD, 2 * HEAD, dtype=wide)
    before = jnp.where(member == 0, eye, total)
    for k in range(1, QUAD):
        piece = lax.dynamic_index_in_dim(came, (member - k) % QUAD, 0, False)
        total = after(piece, total)
        if k < QUAD - 1:
            before = jnp.where(member == k + 1, total, before)
    sent = total.astype(jnp.bfloat16)
    far = [across_quads(sent, "sp_0", k).astype(wide) for k in range(QUAD - 1, 0, -1)]
    reach = far[0][..., HEAD:]
    for piece in far[1:]:
        reach = onto(piece, reach)
    reach = onto(before, reach)
    mine = jnp.concatenate([reach[0], reach[1]], axis=1)
    swapped = shifted(mine.astype(jnp.bfloat16), "sp_1", 1).astype(wide)
    low = jnp.where(core == 0, mine, swapped)
    high = jnp.where(core == 0, swapped, mine)
    every = jnp.stack([low[:, :HEAD], low[:, HEAD:], high[:, :HEAD], high[:, HEAD:]])
    return other.astype(jnp.bfloat16), every


def gathered_weight(weight, behind):
    half = weight.shape[1] // 2
    core = lax.axis_index("sp_1")
    mine = lax.dynamic_slice_in_dim(weight, core * half, half, 1)
    partners = lax.dynamic_slice_in_dim(weight, (1 - core) * half, half, 1)
    mine, behind = lax.optimization_barrier((mine, behind))
    mine = [mine] + [shifted(mine, "tp", k) for k in OFFSETS]
    other = [partners] + [shifted(piece, "sp_1", 1) for piece in mine[1:]]
    return (mine, other), behind


def projected(rows, weights):
    core = lax.axis_index("sp_1")
    halves = [
        sum(jnp.dot(r, w, preferred_element_type=jnp.float32) for r, w in zip(rows, side))
        for side in weights
    ]
    mine, other = halves
    left, right = jnp.where(core == 0, mine, other), jnp.where(core == 0, other, mine)
    return jnp.concatenate([left, right], axis=1)


def own_rows(rows):
    count = lax.axis_size("tp")
    mine = lax.axis_index("tp")
    blocks = rows.reshape(count, -1, rows.shape[1])
    parts = [lax.dynamic_index_in_dim(blocks, mine, 0, False)]
    for k in OFFSETS:
        block = lax.dynamic_index_in_dim(blocks, (mine + k) % count, 0, False)
        parts.append(shifted(block, "tp", k))
    return parts


def split_dot(first, second):
    high_a, high_b = first.astype(jnp.bfloat16), second.astype(jnp.bfloat16)
    low_a = (first - high_a.astype(jnp.float32)).astype(jnp.bfloat16)
    low_b = (second - high_b.astype(jnp.float32)).astype(jnp.bfloat16)
    return plain_dot(high_a, high_b) + (plain_dot(high_a, low_b) + plain_dot(low_a, high_b))


def plain_dot(first, second, dims=((1,), (0,))):
    return lax.dot_general(
        first.astype(jnp.bfloat16),
        second.astype(jnp.bfloat16),
        (dims, ((), ())),
        preferred_element_type=jnp.float32,
    )


def scan_kernel(query_ref, key_ref, value_ref, decay_ref, boost_ref, rate_ref, out_ref, whole_ref):
    wide, narrow = jnp.float32, jnp.bfloat16
    length, width = key_ref.shape
    heads = width // HEAD
    blocks = length // BLK
    keyed = key_ref[...].astype(wide)
    query = query_ref[...].astype(wide)
    valued = value_ref[...]
    lane_r = lax.broadcasted_iota(jnp.int32, (width, width), 0) // HEAD
    lane_c = lax.broadcasted_iota(jnp.int32, (width, width), 1) // HEAD
    same_head = (lane_r == lane_c).astype(narrow)
    square = keyed * keyed
    square_high = square.astype(narrow)
    square_low = (square - square_high.astype(wide)).astype(narrow)
    norm = plain_dot(square_high, same_head) + plain_dot(square_low, same_head)
    unit = keyed * lax.rsqrt(norm + 1e-06)
    insert = unit * jax.nn.sigmoid(rate_ref[...].astype(wide))
    slow = jax.nn.sigmoid(decay_ref[...].astype(wide)) * HALF_DOWN
    log_decay = boost_ref[...] - slow
    row = lax.broadcasted_iota(jnp.int32, (length, length), 0)
    col = lax.broadcasted_iota(jnp.int32, (length, length), 1)
    same_block = row // BLK == col // BLK
    strict = same_block & (row > col)
    inclusive = same_block & (row >= col)
    sums = jnp.concatenate([inclusive.astype(narrow), same_block.astype(narrow)], axis=0)
    part, added = log_decay, 0.0
    for _ in range(3):
        piece = part.astype(narrow)
        added = added + plain_dot(sums, piece)
        part = part - piece.astype(wide)
    upto, final = added[:length], added[length:]
    remove_scaled = -unit * jnp.exp(upto - log_decay)
    query_scaled = query * jnp.exp(upto)
    shrink = jnp.exp(-upto)
    insert_scaled = (insert * shrink).astype(narrow)
    key_scaled = (keyed * shrink).astype(narrow)
    tail = jnp.exp(final - upto)
    insert_tail = (insert * tail).astype(narrow)
    key_tail = (keyed * tail).astype(narrow)
    kept = jnp.exp(final)
    every = range(heads)
    lanes = [slice(h * HEAD, (h + 1) * HEAD) for h in every]
    pair = [
        plain_dot(
            jnp.concatenate([remove_scaled[:, lanes[h]], query_scaled[:, lanes[h]]], axis=0),
            jnp.concatenate([insert_scaled[:, lanes[h]], key_scaled[:, lanes[h]]], axis=0),
            ((1,), (1,)),
        )
        for h in every
    ]
    among = [jnp.where(strict, pair[h][:length, :length], 0.0).astype(narrow) for h in every]
    read = [jnp.where(inclusive, pair[h][length:, :length], 0.0).astype(narrow) for h in every]
    by_keys = [
        jnp.concatenate(
            [
                jnp.where(strict, pair[h][:length, length:], 0.0),
                jnp.where(inclusive, pair[h][length:, length:], 0.0),
            ],
            axis=0,
        ).astype(narrow)
        for h in every
    ]
    from_values = [plain_dot(by_keys[h], valued[:, lanes[h]]) for h in every]
    solved = [
        jnp.concatenate([remove_scaled[:, lanes[h]], from_values[h][:length]], axis=1)
        for h in every
    ]
    power = among
    covered = 1
    while covered < BLK:
        solved = [solved[h] + plain_dot(power[h], solved[h]) for h in every]
        covered = 2 * covered
        if covered < BLK:
            power = [plain_dot(power[h], power[h]).astype(narrow) for h in every]
    reading = [
        jnp.concatenate([query_scaled[:, lanes[h]], from_values[h][length:]], axis=1)
        + plain_dot(read[h], solved[h])
        for h in every
    ]
    wide_r = lax.broadcasted_iota(jnp.int32, (HEAD, 2 * HEAD), 0)
    wide_c = lax.broadcasted_iota(jnp.int32, (HEAD, 2 * HEAD), 1)
    diagonal = wide_r == wide_c
    is_state = wide_c >= HEAD
    none = jnp.zeros((BLK, HEAD), narrow)
    so_far = [None] * heads
    for n in range(blocks):
        rows = slice(n * BLK, (n + 1) * BLK)
        maps = []
        for h in every:
            sources = jnp.concatenate([insert_tail[rows, lanes[h]], key_tail[rows, lanes[h]]], axis=0)
            targets = jnp.concatenate(
                [
                    solved[h][rows].astype(narrow),
                    jnp.concatenate([none, valued[rows, lanes[h]]], axis=1),
                ],
                axis=0,
            )
            keeps = kept[n * BLK : n * BLK + 1, lanes[h]]
            keeps = jnp.concatenate([keeps, keeps], axis=1)
            maps.append(
                plain_dot(sources, targets, ((0,), (0,))) + jnp.where(diagonal, keeps, 0.0)
            )
        for h in every:
            here = reading[h][rows]
            if n == 0:
                out_ref[h, rows, :] = here
                so_far[h] = maps[h]
            else:
                moved = split_dot(here[:, :HEAD], so_far[h])
                local = lax.broadcasted_iota(jnp.int32, here.shape, 1) >= HEAD
                out_ref[h, rows, :] = moved + jnp.where(local, here, 0.0)
                so_far[h] = split_dot(maps[h][:, :HEAD], so_far[h]) + jnp.where(
                    is_state, maps[h], 0.0
                )
    for h in every:
        whole_ref[h] = so_far[h].astype(narrow)


def in_vmem(count):
    return [pl.BlockSpec(memory_space=pltpu.VMEM)] * count


def scanned(*arrays):
    length, width = arrays[0].shape
    heads = width // HEAD
    return pl.pallas_call(
        scan_kernel,
        out_shape=(
            jax.ShapeDtypeStruct((heads, length, 2 * HEAD), jnp.float32),
            jax.ShapeDtypeStruct((heads, HEAD, 2 * HEAD), jnp.bfloat16),
        ),
        in_specs=in_vmem(6),
        out_specs=tuple(in_vmem(2)),
        cost_estimate=pl.CostEstimate(flops=4_000_000_000, bytes_accessed=1 << 20, transcendentals=0),
        name="scan_blocks",
    )(*arrays)


def finish_kernel(core_ref, out_ref, first_ref, reach_ref, gate_ref, gain_ref, gated_ref):
    wide = jnp.float32
    heads = out_ref.shape[0]
    later_core = core_ref[0] > 0
    parts = []
    for h in range(heads):
        before = first_ref[h].astype(wide)
        reach = reach_ref[h]
        passed = split_dot(before[:, :HEAD], reach) + before[:, HEAD:]
        reach = jnp.where(later_core, passed, reach)
        here = out_ref[h]
        mixed = split_dot(here[:, :HEAD], reach) + here[:, HEAD:]
        centre = mixed - jnp.mean(mixed, axis=1, keepdims=True)
        spread = jnp.mean(centre * centre, axis=1, keepdims=True)
        parts.append(centre * lax.rsqrt(spread + 0.00064))
    normed = jnp.concatenate(parts, axis=1) * gain_ref[...]
    gated_ref[...] = (normed * jax.nn.sigmoid(gate_ref[...].astype(wide))).astype(gated_ref.dtype)


def finished(outputs, first, reach, gate_logits, gain):
    core = lax.axis_index("sp_1").astype(jnp.int32).reshape(1)
    return pl.pallas_call(
        finish_kernel,
        out_shape=jax.ShapeDtypeStruct(gate_logits.shape, jnp.bfloat16),
        in_specs=[pl.BlockSpec(memory_space=pltpu.SMEM), *in_vmem(5)],
        out_specs=in_vmem(1)[0],
        cost_estimate=pl.CostEstimate(flops=400_000_000, bytes_accessed=1 << 19, transcendentals=0),
        name="finish_heads",
    )(core, outputs, first, reach, gate_logits, gain.reshape(1, -1))


def hidden_rows(rows, gate, up):
    gated = plain_dot(rows, gate)
    return (gated * jax.nn.sigmoid(gated) * plain_dot(rows, up)).astype(jnp.bfloat16)


def first_kernel(rows, gate, up, down, out, gates, ups, downs, hidden, sems):
    width, width_ff = gate.shape
    cuts = [pl.ds(f, min(FF_TILE, width_ff - f)) for f in range(0, width_ff, FF_TILE)]
    wide_cuts = [pl.ds(f, 2 * FF_TILE) for f in range(0, width, 2 * FF_TILE)]
    copies = []
    for which, (source, here) in enumerate(((gate, gates), (up, ups), (down, downs))):
        places = wide_cuts if which == 2 else cuts
        copies.append(
            [
                pltpu.make_async_copy(source.at[:, p], here.at[:, p], sems.at[which, n])
                for n, p in enumerate(places)
            ]
        )
    for n in range(len(cuts)):
        copies[0][n].start()
        copies[1][n].start()
    for one in copies[2]:
        one.start()
    for n, p in enumerate(cuts):
        copies[0][n].wait()
        copies[1][n].wait()
        hidden[:, p] = hidden_rows(rows[...], gates[:, p], ups[:, p])
    for n, p in enumerate(wide_cuts):
        copies[2][n].wait()
        out[:, p] = plain_dot(hidden[...], downs[:, p]).astype(out.dtype)


def first_rows(rows, gate, up, down):
    count, width = rows.shape
    width_ff = gate.shape[1]
    shapes = [jax.ShapeDtypeStruct(a.shape, a.dtype) for a in (rows, gate, up, down)]
    return pl.pallas_call(
        first_kernel,
        out_shape=tuple(shapes),
        in_specs=[in_vmem(1)[0], *[pl.BlockSpec(memory_space=pltpu.HBM)] * 3],
        out_specs=tuple(in_vmem(4)),
        scratch_shapes=[
            pltpu.VMEM((count, width_ff), jnp.bfloat16),
            pltpu.SemaphoreType.DMA((3, 4)),
        ],
        compiler_params=pltpu.CompilerParams(vmem_limit_bytes=LIMIT_FIRST << 20),
        cost_estimate=pl.CostEstimate(
            flops=6 * count * width * width_ff, bytes_accessed=6 * width * width_ff, transcendentals=0
        ),
        name="first_rows",
    )(rows, gate, up, down)


def more_kernel(count, *refs):
    pieces, (gates, ups, downs), (out, hidden) = refs[:count], refs[count : count + 3], refs[count + 3 :]
    width, width_ff = gates.shape
    rows = pieces[0][...]
    if count > 1:
        rows = jnp.concatenate([piece[...] for piece in pieces], axis=0)
    for f in range(0, width_ff, FF_TILE):
        p = slice(f, min(f + FF_TILE, width_ff))
        hidden[:, p] = hidden_rows(rows, gates[:, p], ups[:, p])
    for f in range(0, width, 2 * FF_TILE):
        p = slice(f, f + 2 * FF_TILE)
        out[:, p] = plain_dot(hidden[...], downs[:, p]).astype(out.dtype)


def more_rows(pieces, weights):
    count, width = sum(piece.shape[0] for piece in pieces), pieces[0].shape[1]
    width_ff = weights[0].shape[1]
    return pl.pallas_call(
        partial(more_kernel, len(pieces)),
        out_shape=jax.ShapeDtypeStruct((count, width), jnp.bfloat16),
        in_specs=in_vmem(len(pieces) + 3),
        out_specs=in_vmem(1)[0],
        scratch_shapes=[pltpu.VMEM((count, width_ff), jnp.bfloat16)],
        compiler_params=pltpu.CompilerParams(vmem_limit_bytes=LIMIT_REST << 20),
        cost_estimate=pl.CostEstimate(
            flops=6 * count * width * width_ff, bytes_accessed=6 * width * width_ff, transcendentals=0
        ),
        name="more_rows",
    )(*pieces, *weights)


def body(
    receptance,
    head_keys,
    head_values,
    decay_logits,
    decay_boost,
    correction_logits,
    gate_logits,
    head_norm_gain,
    output_weight,
    residual,
    expert_norm_gain,
    routes,
    routing_weight,
    expert_gate_weight,
    expert_up_weight,
    expert_down_weight,
):
    outputs, whole = scanned(
        receptance, head_keys, head_values, decay_logits, decay_boost, correction_logits
    )
    weights, whole = gathered_weight(output_weight, whole)
    first, reach = incoming_state(whole)
    gated = finished(outputs, first, reach, gate_logits, head_norm_gain)
    rows_here = own_rows(gated)
    branch = projected(rows_here, weights)
    stream = residual.astype(jnp.float32) + branch
    normal = (
        stream
        * lax.rsqrt(jnp.mean(stream * stream, axis=-1, keepdims=True) + 1e-06)
        * expert_norm_gain
    ).astype(jnp.bfloat16)
    sp_count = lax.axis_size(SP)
    tp_count = lax.axis_size("tp")
    capacity = max(2, 2 * TOK_DEV * TOP // (tp_count * sp_count))
    local_count = normal.shape[0]
    width_model = normal.shape[1]
    flat_routes = routes.reshape(-1)
    expert_ids = jnp.arange(sp_count, dtype=jnp.int32)
    chosen = (flat_routes[:, None] == expert_ids[None, :]).astype(jnp.int32)
    earlier = jnp.cumsum(chosen, axis=0) - chosen
    rank = jnp.sum(earlier * chosen, axis=1)
    place = flat_routes * capacity + rank
    places = jnp.arange(sp_count * capacity, dtype=jnp.int32)
    onehot = (place[:, None] == places[None, :]).astype(jnp.bfloat16)
    placed = jnp.sum(onehot.reshape(local_count, TOP, sp_count * capacity), axis=1)
    placed, onehot, routing_weight = lax.optimization_barrier((placed, onehot, routing_weight))
    outbound = jnp.einsum("ts,td->sd", placed, normal, preferred_element_type=jnp.float32).astype(
        jnp.bfloat16
    )
    going = outbound.reshape(sp_count, 2 * capacity, width_model // 2)
    arrived = lax.all_to_all(going, SP, split_axis=0, concat_axis=0, tiled=True)
    arrived = arrived.reshape(-1, width_model)
    back, ahead = shifted(arrived, "tp", 1), shifted(arrived, "tp", -1)
    weights = (expert_gate_weight[0], expert_up_weight[0], expert_down_weight[0])
    own, *weights = first_rows(arrived, *weights)
    middle = arrived.shape[0] // 2
    away = [shifted(back[:middle], "tp", 1), shifted(ahead[middle:], "tp", -1)]
    back = more_rows([back], weights)
    ahead = more_rows([ahead], weights)
    away = more_rows(away, weights)
    parts = [own]
    for piece, k in ((back, -1), (ahead, 1), (away, 2)):
        parts.append(shifted(piece, "tp", k))
    total = sum(piece.astype(jnp.float32) for piece in parts).astype(jnp.bfloat16)
    total = total.reshape(sp_count, 2 * capacity, width_model // 2)
    home = lax.all_to_all(total, SP, split_axis=0, concat_axis=0, tiled=True)
    home = home.reshape(-1, width_model)
    picked = jnp.dot(onehot, home, preferred_element_type=jnp.float32)
    routed = jnp.sum(
        picked.reshape(local_count, TOP, width_model) * routing_weight[:, :, None], axis=1
    )
    return (stream + routed).astype(jnp.bfloat16)


def solution(mesh):
    torus = Mesh(
        mesh.devices.reshape(mesh.shape["grp"], 16, 2, mesh.shape["tp"]),
        ("grp", "sp_0", "sp_1", "tp"),
    )
    return jax.shard_map(
        body,
        mesh=torus,
        in_specs=(
            P(GRP_SP, "tp"),
            P(GRP_SP, "tp"),
            P(GRP_SP, "tp"),
            P(GRP_SP, "tp"),
            P(GRP_SP, "tp"),
            P(GRP_SP, "tp"),
            P(GRP_SP, "tp"),
            P("tp"),
            P("tp", None),
            P(GRP_SP_TP, None),
            P(),
            P(GRP_SP_TP, None),
            P(GRP_SP_TP, None),
            P(SP, None, "tp"),
            P(SP, None, "tp"),
            P(SP, "tp", None),
        ),
        out_specs=P(GRP_SP_TP, None),
        check_vma=False,
    )
```

profile of v0, /device:TPU:40, one launch (start us, length us, event | category | flops | bytes accessed | tf_op | source)
XLA Modules:
  0.0 215.7 jit_solution(12284975988018049292)
XLA Ops:
  0.0 1.2 copy-done
  1.3 4.1 %scan_blocks.1 = (f32[4,128,128]{2,1,0:T(8,128)}, bf16[4,64,128]{2,1,0:T(8,128)(2,1)}) custom-call(bf16[128,256]{1,0:T(8,128)(2,1)} %query_ref.1, bf16[128,256]{1,0:T(8,128)(2,1)} %key_ref.1, bf16[128,256]{1,0:T(8,128)(2,1)} %value_ref.1, bf16[128,256]{1,0:T(8,128)(2,1)} %decay_ref.1, f32[128,256]{1,0:T(8,128)} %boost_ref.1, bf16[128,256]{1,0:T(8,128)(2,1)} %rate_ref.1), custom_call_target="tpu_custom_call" | custom-call | flops 4000000000 | bytes 1048576 | tf_op jit(solution)/shard_map/scan_blocks/pallas_call | solution.py:269
  5.4 3.3 %collective-permute-start.13 = (bf16[256,1024]{1,0:T(8,128)(2,1)S(1)}, bf16[256,1024]{1,0:T(8,128)(2,1)S(1)}, u32[]{:S(2)}, u32[]{:S(2)}) collective-permute-start(bf16[256,1024]{1,0:T(8,128)(2,1)S(1)} %constant_dynamic-slice_fusion), channel_id=1, source_target_pairs={{0,2},{1,3},{2,0},{3,1},{4,6},{5,7},{6,4},{7,5},{8,10},{9,11},{10,... | collective-permute-start | bytes 1572872 | tf_op jit(solution)/shard_map/ppermute | solution.py:33
  8.7 1.0 collective-permute-start.11
  9.7 1.0 collective-permute-start.9
  13.5 1.5 fusion.40
  15.0 7.2 %collective-permute-start.3 = (bf16[2,64,128]{2,1,0:T(8,128)(2,1)}, bf16[2,64,128]{2,1,0:T(8,128)(2,1)S(1)}, u32[]{:S(2)}, u32[]{:S(2)}) collective-permute-start(bf16[2,64,128]{2,1,0:T(8,128)(2,1)} %get-tuple-element.43), channel_id=1, source_target_pairs={{0,24},{8,0},{16,8},{24,16},{32,56},{40,32},{48,40},{56,48},{64,88... | collective-permute-start | bytes 98312 | tf_op jit(solution)/shard_map/ppermute | solution.py:39
  24.7 4.8 %collective-permute-done.2 = bf16[2,64,128]{2,1,0:T(8,128)(2,1)S(1)} collective-permute-done((bf16[2,64,128]{2,1,0:T(8,128)(2,1)}, bf16[2,64,128]{2,1,0:T(8,128)(2,1)S(1)}, u32[]{:S(2)}, u32[]{:S(2)}) %collective-permute-start.2) | collective-permute-done | bytes 32800 | tf_op jit(solution)/shard_map/ppermute | solution.py:39
  31.2 1.0 fusion.15
  33.0 20.4 %collective-permute-start.6 = (bf16[2,64,128]{2,1,0:T(8,128)(2,1)S(1)}, bf16[2,64,128]{2,1,0:T(8,128)(2,1)S(1)}, u32[]{:S(2)}, u32[]{:S(2)}) collective-permute-start(bf16[2,64,128]{2,1,0:T(8,128)(2,1)S(1)} %fusion.3), channel_id=1, source_target_pairs={{0,96},{8,104},{16,112},{24,120},{1,97},{9,105},{17,113},{25,121},... | collective-permute-start | bytes 98312 | tf_op jit(solution)/shard_map/ppermute | solution.py:44
  53.4 1.3 collective-permute-start.5
  55.9 6.8 %collective-permute-start.4 = (bf16[2,64,128]{2,1,0:T(8,128)(2,1)S(1)}, bf16[2,64,128]{2,1,0:T(8,128)(2,1)S(1)}, u32[]{:S(2)}, u32[]{:S(2)}) collective-permute-start(bf16[2,64,128]{2,1,0:T(8,128)(2,1)S(1)} %fusion.3), channel_id=1, source_target_pairs={{0,32},{8,40},{16,48},{24,56},{32,64},{40,72},{48,80},{56,88},{64,... | collective-permute-start | bytes 98312 | tf_op jit(solution)/shard_map/ppermute | solution.py:44
  62.9 1.4 collective-permute-done.4
  66.8 2.5 %finish_heads.1 = bf16[128,256]{1,0:T(8,128)(2,1)} custom-call(s32[1]{0:T(128)} %bitcast.core_ref, f32[4,128,128]{2,1,0:T(8,128)} %get-tuple-element.16.out_ref, bf16[4,64,128]{2,1,0:T(8,128)(2,1)} %copy-done.2, f32[4,64,64]{2,1,0:T(8,128)} %pad_maximum_fusion.1.reach_ref, bf16[128,256]{1,0:T(8,128)(2,1)} %gate_ref.1, f32[1,256]{1,0:T(1,128)} %bitcast.81), custom_call_target="tpu_custom_call" | custom-call | flops 400000000 | bytes 524288 | tf_op jit(solution)/shard_map/finish_heads/pallas_call | solution.py:303
  70.1 2.2 %collective-permute-start.10 = (bf16[32,256]{1,0:T(8,128)(2,1)S(1)}, bf16[32,256]{1,0:T(8,128)(2,1)S(1)}, u32[]{:S(2)}, u32[]{:S(2)}) collective-permute-start(bf16[32,256]{1,0:T(8,128)(2,1)S(1)} %get-tuple-element.34), channel_id=1, source_target_pairs={{0,3},{1,0},{2,1},{3,2},{4,7},{5,4},{6,5},{7,6},{8,11},{9,8},{10,9... | collective-permute-start | bytes 49160 | tf_op jit(solution)/shard_map/ppermute | solution.py:33
  73.3 4.0 %collective-permute-done.8 = bf16[32,256]{1,0:T(8,128)(2,1)S(1)} collective-permute-done((bf16[32,256]{1,0:T(8,128)(2,1)S(1)}, bf16[32,256]{1,0:T(8,128)(2,1)S(1)}, u32[]{:S(2)}, u32[]{:S(2)}) %collective-permute-start.8) | collective-permute-done | bytes 16416 | tf_op jit(solution)/shard_map/ppermute | solution.py:33
  77.5 0.9 convolution_add_fusion.3
  79.0 3.5 %collective-permute-done.12 = bf16[32,256]{1,0:T(8,128)(2,1)S(1)} collective-permute-done((bf16[32,256]{1,0:T(8,128)(2,1)S(1)}, bf16[32,256]{1,0:T(8,128)(2,1)S(1)}, u32[]{:S(2)}, u32[]{:S(2)}) %collective-permute-start.12) | collective-permute-done | bytes 16416 | tf_op jit(solution)/shard_map/ppermute | solution.py:33
  83.5 1.3 collective-permute-done.15
  85.7 43.2 %all_to_all.10 = bf16[32,8,1024]{2,1,0:T(8,128)(2,1)S(1)} all-to-all(bf16[32,8,1024]{2,1,0:T(8,128)(2,1)S(1)} %reshape.56), channel_id=1, replica_groups=mesh['grp'=2,'sp_0'=16,'sp_1'=2,'tp'=4] {'sp_0','sp_1'}, dimensions={0} | all-to-all | bytes 1048576 | tf_op jit(solution)/shard_map/all_to_all | solution.py:448
  129.2 2.0 collective-permute-start.17
  131.2 5.1 %first_rows.1 = (bf16[128,2048]{1,0:T(8,128)(2,1)S(1)}, bf16[2048,896]{1,0:T(8,128)(2,1)S(1)}, bf16[2048,896]{1,0:T(8,128)(2,1)S(1)}, bf16[896,2048]{1,0:T(8,128)(2,1)S(1)}) custom-call(bf16[128,2048]{1,0:T(8,128)(2,1)S(1)} %reshape.57.rows, bf16[2048,896]{1,0:T(8,128)(2,1)} %bitcast.73, bf16[2048,896]{1,0:T(8,128)(2,1)} %bitcast.74, bf16[896,2048]{1,0:T(8,128)(2,1)} %bitcast.75), custom_call_target="tpu_custom_call" | custom-call | flops 1409286144 | bytes 11010048 | tf_op jit(solution)/shard_map/first_rows/pallas_call | solution.py:349
  136.3 6.7 %collective-permute-done.19.refs_0_ = bf16[128,2048]{1,0:T(8,128)(2,1)S(1)} collective-permute-done((bf16[128,2048]{1,0:T(8,128)(2,1)S(1)}, bf16[128,2048]{1,0:T(8,128)(2,1)S(1)}, u32[]{:S(2)}, u32[]{:S(2)}) %collective-permute-start.19) | collective-permute-done | bytes 524320 | tf_op jit(solution)/shard_map/ppermute | solution.py:33
  143.0 1.6 collective-permute-start.22
  145.3 1.8 more_rows.3
  147.1 3.1 %collective-permute-start.18 = (bf16[128,2048]{1,0:T(8,128)(2,1)S(1)}, bf16[128,2048]{1,0:T(8,128)(2,1)S(1)}, u32[]{:S(2)}, u32[]{:S(2)}) collective-permute-start(bf16[128,2048]{1,0:T(8,128)(2,1)S(1)} %more_rows.3), channel_id=1, source_target_pairs={{0,3},{1,0},{2,1},{3,2},{4,7},{5,4},{6,5},{7,6},{8,11},{9,8},{10,9... | collective-permute-start | bytes 1572872 | tf_op jit(solution)/shard_map/ppermute | solution.py:33
  150.2 1.8 more_rows.4
  152.3 1.1 collective-permute-done.21.refs_0_
  153.4 1.8 more_rows.5
  155.6 16.8 %collective-permute-done.18 = bf16[128,2048]{1,0:T(8,128)(2,1)S(1)} collective-permute-done((bf16[128,2048]{1,0:T(8,128)(2,1)S(1)}, bf16[128,2048]{1,0:T(8,128)(2,1)S(1)}, u32[]{:S(2)}, u32[]{:S(2)}) %collective-permute-start.18) | collective-permute-done | bytes 524320 | tf_op jit(solution)/shard_map/ppermute | solution.py:33
  172.3 4.7 %collective-permute-done.20 = bf16[128,2048]{1,0:T(8,128)(2,1)S(1)} collective-permute-done((bf16[128,2048]{1,0:T(8,128)(2,1)S(1)}, bf16[128,2048]{1,0:T(8,128)(2,1)S(1)}, u32[]{:S(2)}, u32[]{:S(2)}) %collective-permute-start.20) | collective-permute-done | bytes 524320 | tf_op jit(solution)/shard_map/ppermute | solution.py:33
  177.5 37.1 %all_to_all.11 = bf16[32,8,1024]{2,1,0:T(8,128)(2,1)S(1)} all-to-all(bf16[32,8,1024]{2,1,0:T(8,128)(2,1)S(1)} %reshape.58), channel_id=1, replica_groups=mesh['grp'=2,'sp_0'=16,'sp_1'=2,'tp'=4] {'sp_0','sp_1'}, dimensions={0} | all-to-all | bytes 1048576 | tf_op jit(solution)/shard_map/all_to_all | solution.py:463
  (95 shorter events, 19.2 us)
Async XLA Ops:
  0.0 1.2 copy-start
  1.3 10.3 %copy-start.5 = (s32[32,2]{0,1:T(2,128)S(1)}, s32[32,2]{0,1:T(2,128)}, u32[]{:S(2)}) copy-start(s32[32,2]{0,1:T(2,128)} %param.27) | copy-start | bytes 772
  5.4 71.9 %collective-permute-start.13 = (bf16[256,1024]{1,0:T(8,128)(2,1)S(1)}, bf16[256,1024]{1,0:T(8,128)(2,1)S(1)}, u32[]{:S(2)}, u32[]{:S(2)}) collective-permute-start(bf16[256,1024]{1,0:T(8,128)(2,1)S(1)} %constant_dynamic-slice_fusion), channel_id=1, source_target_pairs={{0,2},{1,3},{2,0},{3,1},{4,6},{5,7},{6,4},{7,5},{8,10},{9,11},{10,... | collective-permute-start | bytes 1572872 | tf_op jit(solution)/shard_map/ppermute | solution.py:33
  8.7 74.0 %collective-permute-start.11 = (bf16[256,1024]{1,0:T(8,128)(2,1)S(1)}, bf16[256,1024]{1,0:T(8,128)(2,1)S(1)}, u32[]{:S(2)}, u32[]{:S(2)}) collective-permute-start(bf16[256,1024]{1,0:T(8,128)(2,1)S(1)} %constant_dynamic-slice_fusion), channel_id=1, source_target_pairs={{0,3},{1,0},{2,1},{3,2},{4,7},{5,4},{6,5},{7,6},{8,11},{9,8},{10,9... | collective-permute-start | bytes 1572872 | tf_op jit(solution)/shard_map/ppermute | solution.py:33
  9.7 67.6 %collective-permute-start.9 = (bf16[256,1024]{1,0:T(8,128)(2,1)S(1)}, bf16[256,1024]{1,0:T(8,128)(2,1)S(1)}, u32[]{:S(2)}, u32[]{:S(2)}) collective-permute-start(bf16[256,1024]{1,0:T(8,128)(2,1)S(1)} %constant_dynamic-slice_fusion), channel_id=1, source_target_pairs={{0,1},{1,2},{2,3},{3,0},{4,5},{5,6},{6,7},{7,4},{8,9},{9,10},{10,1... | collective-permute-start | bytes 1572872 | tf_op jit(solution)/shard_map/ppermute | solution.py:33
  10.7 2.1 collective-permute-start
  12.1 1.3 copy-start.6
  12.8 0.6 copy-start.2
  15.0 9.2 %collective-permute-start.3 = (bf16[2,64,128]{2,1,0:T(8,128)(2,1)}, bf16[2,64,128]{2,1,0:T(8,128)(2,1)S(1)}, u32[]{:S(2)}, u32[]{:S(2)}) collective-permute-start(bf16[2,64,128]{2,1,0:T(8,128)(2,1)} %get-tuple-element.43), channel_id=1, source_target_pairs={{0,24},{8,0},{16,8},{24,16},{32,56},{40,32},{48,40},{56,48},{64,88... | collective-permute-start | bytes 98312 | tf_op jit(solution)/shard_map/ppermute | solution.py:39
  24.2 5.4 %collective-permute-start.2 = (bf16[2,64,128]{2,1,0:T(8,128)(2,1)}, bf16[2,64,128]{2,1,0:T(8,128)(2,1)S(1)}, u32[]{:S(2)}, u32[]{:S(2)}) collective-permute-start(bf16[2,64,128]{2,1,0:T(8,128)(2,1)} %get-tuple-element.43), channel_id=1, source_target_pairs={{0,16},{8,24},{16,0},{24,8},{32,48},{40,56},{48,32},{56,40},{64,80... | collective-permute-start | bytes 98312 | tf_op jit(solution)/shard_map/ppermute | solution.py:39
  24.2 6.1 %collective-permute-start.1 = (bf16[2,64,128]{2,1,0:T(8,128)(2,1)}, bf16[2,64,128]{2,1,0:T(8,128)(2,1)S(1)}, u32[]{:S(2)}, u32[]{:S(2)}) collective-permute-start(bf16[2,64,128]{2,1,0:T(8,128)(2,1)} %get-tuple-element.43), channel_id=1, source_target_pairs={{0,8},{8,16},{16,24},{24,0},{32,40},{40,48},{48,56},{56,32},{64,72... | collective-permute-start | bytes 98312 | tf_op jit(solution)/shard_map/ppermute | solution.py:39
  33.0 22.9 %collective-permute-start.6 = (bf16[2,64,128]{2,1,0:T(8,128)(2,1)S(1)}, bf16[2,64,128]{2,1,0:T(8,128)(2,1)S(1)}, u32[]{:S(2)}, u32[]{:S(2)}) collective-permute-start(bf16[2,64,128]{2,1,0:T(8,128)(2,1)S(1)} %fusion.3), channel_id=1, source_target_pairs={{0,96},{8,104},{16,112},{24,120},{1,97},{9,105},{17,113},{25,121},... | collective-permute-start | bytes 98312 | tf_op jit(solution)/shard_map/ppermute | solution.py:44
  53.4 9.3 %collective-permute-start.5 = (bf16[2,64,128]{2,1,0:T(8,128)(2,1)S(1)}, bf16[2,64,128]{2,1,0:T(8,128)(2,1)S(1)}, u32[]{:S(2)}, u32[]{:S(2)}) collective-permute-start(bf16[2,64,128]{2,1,0:T(8,128)(2,1)S(1)} %fusion.3), channel_id=1, source_target_pairs={{0,64},{8,72},{16,80},{24,88},{32,96},{40,104},{48,112},{56,120},{... | collective-permute-start | bytes 98312 | tf_op jit(solution)/shard_map/ppermute | solution.py:44
  55.9 8.4 %collective-permute-start.4 = (bf16[2,64,128]{2,1,0:T(8,128)(2,1)S(1)}, bf16[2,64,128]{2,1,0:T(8,128)(2,1)S(1)}, u32[]{:S(2)}, u32[]{:S(2)}) collective-permute-start(bf16[2,64,128]{2,1,0:T(8,128)(2,1)S(1)} %fusion.3), channel_id=1, source_target_pairs={{0,32},{8,40},{16,48},{24,56},{32,64},{40,72},{48,80},{56,88},{64,... | collective-permute-start | bytes 98312 | tf_op jit(solution)/shard_map/ppermute | solution.py:44
  64.7 1.2 collective-permute-start.7
  66.8 18.2 %copy-start.1 = (bf16[32,2048]{1,0:T(8,128)(2,1)S(1)}, bf16[32,2048]{1,0:T(8,128)(2,1)}, u32[]{:S(2)}) copy-start(bf16[32,2048]{1,0:T(8,128)(2,1)} %param.25) | copy-start | bytes 393220
  69.3 15.8 %copy-start.3 = (bf16[32,128]{1,0:T(8,128)(2,1)S(1)}, bf16[32,128]{1,0:T(8,128)(2,1)}, u32[]{:S(2)}) copy-start(bf16[32,128]{1,0:T(8,128)(2,1)} %fusion.28) | copy-start | bytes 24580
  69.3 15.8 %copy-start.4 = (f32[2048]{0:T(1024)S(1)}, f32[2048]{0:T(1024)}, u32[]{:S(2)}) copy-start(f32[2048]{0:T(1024)} %param.26) | copy-start | bytes 24580
  70.1 12.8 %collective-permute-start.10 = (bf16[32,256]{1,0:T(8,128)(2,1)S(1)}, bf16[32,256]{1,0:T(8,128)(2,1)S(1)}, u32[]{:S(2)}, u32[]{:S(2)}) collective-permute-start(bf16[32,256]{1,0:T(8,128)(2,1)S(1)} %get-tuple-element.34), channel_id=1, source_target_pairs={{0,3},{1,0},{2,1},{3,2},{4,7},{5,4},{6,5},{7,6},{8,11},{9,8},{10,9... | collective-permute-start | bytes 49160 | tf_op jit(solution)/shard_map/ppermute | solution.py:33
  72.3 4.9 %collective-permute-start.8 = (bf16[32,256]{1,0:T(8,128)(2,1)S(1)}, bf16[32,256]{1,0:T(8,128)(2,1)S(1)}, u32[]{:S(2)}, u32[]{:S(2)}) collective-permute-start(bf16[32,256]{1,0:T(8,128)(2,1)S(1)} %get-tuple-element.36), channel_id=1, source_target_pairs={{0,1},{1,2},{2,3},{3,0},{4,5},{5,6},{6,7},{7,4},{8,9},{9,10},{10,1... | collective-permute-start | bytes 49160 | tf_op jit(solution)/shard_map/ppermute | solution.py:33
  77.3 5.2 %collective-permute-start.12 = (bf16[32,256]{1,0:T(8,128)(2,1)S(1)}, bf16[32,256]{1,0:T(8,128)(2,1)S(1)}, u32[]{:S(2)}, u32[]{:S(2)}) collective-permute-start(bf16[32,256]{1,0:T(8,128)(2,1)S(1)} %get-tuple-element.35), channel_id=1, source_target_pairs={{0,2},{1,3},{2,0},{3,1},{4,6},{5,7},{6,4},{7,5},{8,10},{9,11},{10,... | collective-permute-start | bytes 49160 | tf_op jit(solution)/shard_map/ppermute | solution.py:33
  77.3 5.8 %collective-permute-start.16 = (bf16[256,1024]{1,0:T(8,128)(2,1)S(1)}, bf16[256,1024]{1,0:T(8,128)(2,1)S(1)}, u32[]{:S(2)}, u32[]{:S(2)}) collective-permute-start(bf16[256,1024]{1,0:T(8,128)(2,1)S(1)} %collective-permute-done.13), channel_id=1, source_target_pairs={{0,4},{4,0},{1,5},{5,1},{2,6},{6,2},{3,7},{7,3},{8,12},{12,8},{9,1... | collective-permute-start | bytes 1572872 | tf_op jit(solution)/shard_map/ppermute | solution.py:33
  78.4 4.9 %collective-permute-start.14 = (bf16[256,1024]{1,0:T(8,128)(2,1)S(1)}, bf16[256,1024]{1,0:T(8,128)(2,1)S(1)}, u32[]{:S(2)}, u32[]{:S(2)}) collective-permute-start(bf16[256,1024]{1,0:T(8,128)(2,1)S(1)} %collective-permute-done.9), channel_id=1, source_target_pairs={{0,4},{4,0},{1,5},{5,1},{2,6},{6,2},{3,7},{7,3},{8,12},{12,8},{9,1... | collective-permute-start | bytes 1572872 | tf_op jit(solution)/shard_map/ppermute | solution.py:33
  82.7 2.0 collective-permute-start.15
  129.1 13.9 %collective-permute-start.19 = (bf16[128,2048]{1,0:T(8,128)(2,1)S(1)}, bf16[128,2048]{1,0:T(8,128)(2,1)S(1)}, u32[]{:S(2)}, u32[]{:S(2)}) collective-permute-start(bf16[128,2048]{1,0:T(8,128)(2,1)S(1)} %reshape.57.rows), channel_id=1, source_target_pairs={{0,3},{1,0},{2,1},{3,2},{4,7},{5,4},{6,5},{7,6},{8,11},{9,8},{10,9... | collective-permute-start | bytes 1572872 | tf_op jit(solution)/shard_map/ppermute | solution.py:33
  129.2 15.5 %collective-permute-start.17 = (bf16[128,2048]{1,0:T(8,128)(2,1)S(1)}, bf16[128,2048]{1,0:T(8,128)(2,1)S(1)}, u32[]{:S(2)}, u32[]{:S(2)}) collective-permute-start(bf16[128,2048]{1,0:T(8,128)(2,1)S(1)} %reshape.57.rows), channel_id=1, source_target_pairs={{0,1},{1,2},{2,3},{3,0},{4,5},{5,6},{6,7},{7,4},{8,9},{9,10},{10,1... | collective-permute-start | bytes 1572872 | tf_op jit(solution)/shard_map/ppermute | solution.py:33
  143.0 9.3 %collective-permute-start.22 = (bf16[64,2048]{1,0:T(8,128)(2,1)S(1)}, bf16[64,2048]{1,0:T(8,128)(2,1)S(1)}, u32[]{:S(2)}, u32[]{:S(2)}) collective-permute-start(bf16[64,2048]{1,0:T(8,128)(2,1)S(1)} %slice.102), channel_id=1, source_target_pairs={{0,3},{1,0},{2,1},{3,2},{4,7},{5,4},{6,5},{7,6},{8,11},{9,8},{10,9... | collective-permute-start | bytes 786440 | tf_op jit(solution)/shard_map/ppermute | solution.py:33
  144.7 8.7 %collective-permute-start.21 = (bf16[64,2048]{1,0:T(8,128)(2,1)S(1)}, bf16[64,2048]{1,0:T(8,128)(2,1)S(1)}, u32[]{:S(2)}, u32[]{:S(2)}) collective-permute-start(bf16[64,2048]{1,0:T(8,128)(2,1)S(1)} %slice.101), channel_id=1, source_target_pairs={{0,1},{1,2},{2,3},{3,0},{4,5},{5,6},{6,7},{7,4},{8,9},{9,10},{10,1... | collective-permute-start | bytes 786440 | tf_op jit(solution)/shard_map/ppermute | solution.py:33
  147.1 25.2 %collective-permute-start.18 = (bf16[128,2048]{1,0:T(8,128)(2,1)S(1)}, bf16[128,2048]{1,0:T(8,128)(2,1)S(1)}, u32[]{:S(2)}, u32[]{:S(2)}) collective-permute-start(bf16[128,2048]{1,0:T(8,128)(2,1)S(1)} %more_rows.3), channel_id=1, source_target_pairs={{0,3},{1,0},{2,1},{3,2},{4,7},{5,4},{6,5},{7,6},{8,11},{9,8},{10,9... | collective-permute-start | bytes 1572872 | tf_op jit(solution)/shard_map/ppermute | solution.py:33
  152.0 25.0 %collective-permute-start.20 = (bf16[128,2048]{1,0:T(8,128)(2,1)S(1)}, bf16[128,2048]{1,0:T(8,128)(2,1)S(1)}, u32[]{:S(2)}, u32[]{:S(2)}) collective-permute-start(bf16[128,2048]{1,0:T(8,128)(2,1)S(1)} %more_rows.4), channel_id=1, source_target_pairs={{0,1},{1,2},{2,3},{3,0},{4,5},{5,6},{6,7},{7,4},{8,9},{9,10},{10,1... | collective-permute-start | bytes 1572872 | tf_op jit(solution)/shard_map/ppermute | solution.py:33
  155.2 59.6 %copy-start.7 = (f32[32,2]{0,1:T(2,128)S(1)}, f32[32,2]{0,1:T(2,128)}, u32[]{:S(2)}) copy-start(f32[32,2]{0,1:T(2,128)} %param.28) | copy-start | bytes 772
  155.2 21.8 %collective-permute-start.23 = (bf16[128,2048]{1,0:T(8,128)(2,1)S(1)}, bf16[128,2048]{1,0:T(8,128)(2,1)S(1)}, u32[]{:S(2)}, u32[]{:S(2)}) collective-permute-start(bf16[128,2048]{1,0:T(8,128)(2,1)S(1)} %more_rows.5), channel_id=1, source_target_pairs={{0,2},{1,3},{2,0},{3,1},{4,6},{5,7},{6,4},{7,5},{8,10},{9,11},{10,... | collective-permute-start | bytes 1572872 | tf_op jit(solution)/shard_map/ppermute | solution.py:33
where the time goes:
time: 217 us; the launch traced here: 216 us
  blocking collectives  80.2 us (37%)
  starting transfers between devices  52.6 us (24%)
  waiting for transfers between devices  45.9 us (21%)
  Pallas kernels  17.2 us (8%)
  matrix products  8.31 us (4%)
  other arithmetic  5.91 us (3%)
  local copies, waits for them, and re-layouts  5.08 us (2%)
    all_to_all x1, blocking collectives, body(): arrived = lax.all_to_all(going, SP, split_axis=0, concat_axis=0, tiled=True)  43.2 us
    ppermute x18, waiting for transfers between devices, shifted(): return lax.ppermute(x, axis, [(i, (i + step) % size) for i in range(size)])  38.6 us
    all_to_all x1, blocking collectives, body(): home = lax.all_to_all(total, SP, split_axis=0, concat_axis=0, tiled=True)  37.1 us
    ppermute x3, starting transfers between devices, across_quads(): lax.ppermute(x, axis, [(i, i + step * QUAD) for i in range(size - step *...  28.5 us
    ppermute x18, starting transfers between devices, shifted(): return lax.ppermute(x, axis, [(i, (i + step) % size) for i in range(size)])  16.3 us
    ppermute x3, starting transfers between devices, within_quads(): return lax.ppermute(x, axis, pairs)  7.77 us
    ppermute x3, waiting for transfers between devices, within_quads(): return lax.ppermute(x, axis, pairs)  5.47 us
    pallas_call x3, Pallas kernels, more_rows(): pl.pallas_call(partial(more_kernel, len(pieces)), out_shape=jax.ShapeDtyp...  5.43 us
  transfers between devices with their start and end apart: 24, of which 13 were waited for; matrix products, arithmetic and copies ran while one was open for 7% of the time, Pallas kernels for 6%

commit v1 on v0

--- a/solution.py
+++ b/solution.py
@@ -54,19 +54,44 @@
     return moved + later[..., HEAD:]
 
 
+def chip_kernel(core_ref, own_ref, other_ref, chip_ref, sent_ref):
+    core = core_ref[0]
+    half = chip_ref.shape[0]
+    for h in range(half):
+        own = own_ref[core * half + h].astype(jnp.float32)
+        other = other_ref[core * half + h].astype(jnp.float32)
+        first = jnp.where(core == 0, own, other)
+        second = jnp.where(core == 0, other, own)
+        state = lax.broadcasted_iota(jnp.int32, second.shape, 1) >= HEAD
+        chip = split_dot(second[:, :HEAD], first) + jnp.where(state, second, 0.0)
+        chip_ref[h] = chip
+        sent_ref[h] = chip.astype(sent_ref.dtype)
+
+
+def core_index():
+    return lax.axis_index("sp_1").astype(jnp.int32).reshape(1)
+
+
+def chip_map(own, other):
+    shape = (own.shape[0] // 2, *own.shape[1:])
+    return pl.pallas_call(
+        chip_kernel,
+        out_shape=(
+            jax.ShapeDtypeStruct(shape, jnp.float32),
+            jax.ShapeDtypeStruct(shape, jnp.bfloat16),
+        ),
+        in_specs=[pl.BlockSpec(memory_space=pltpu.SMEM), *in_vmem(2)],
+        out_specs=tuple(in_vmem(2)),
+        cost_estimate=pl.CostEstimate(flops=200_000_000, bytes_accessed=1 << 18, transcendentals=0),
+        compiler_params=pltpu.CompilerParams(vmem_limit_bytes=8 << 20),
+        name="chip_map",
+    )(core_index(), own, other)
+
+
 def incoming_state(packed):
     wide = jnp.float32
-    core = lax.axis_index("sp_1")
-    own = packed.astype(wide)
-    other = shifted(packed, "sp_1", 1).astype(wide)
-    first = jnp.where(core == 0, own, other)
-    second = jnp.where(core == 0, other, own)
-    half = own.shape[0] // 2
-    chip = after(
-        lax.dynamic_slice_in_dim(second, core * half, half, 0),
-        lax.dynamic_slice_in_dim(first, core * half, half, 0),
-    )
-    sent = chip.astype(jnp.bfloat16)
+    other = shifted(packed, "sp_1", 1)
+    chip, sent = chip_map(packed, other)
     member = lax.axis_index("sp_0") % QUAD
     came = [chip] + [within_quads(sent, "sp_0", k).astype(wide) for k in range(1, QUAD)]
     came = jnp.stack(came)
@@ -84,45 +109,18 @@
     for piece in far[1:]:
         reach = onto(piece, reach)
     reach = onto(before, reach)
-    mine = jnp.concatenate([reach[0], reach[1]], axis=1)
-    swapped = shifted(mine.astype(jnp.bfloat16), "sp_1", 1).astype(wide)
-    low = jnp.where(core == 0, mine, swapped)
-    high = jnp.where(core == 0, swapped, mine)
-    every = jnp.stack([low[:, :HEAD], low[:, HEAD:], high[:, :HEAD], high[:, HEAD:]])
-    return other.astype(jnp.bfloat16), every
-
-
-def gathered_weight(weight, behind):
+    mine = jnp.concatenate([reach[0], reach[1]], axis=1).astype(jnp.bfloat16)
+    swapped = shifted(mine, "sp_1", 1)
+    return other, mine, swapped
+
+
+def gathered_weight(weight):
     half = weight.shape[1] // 2
     core = lax.axis_index("sp_1")
     mine = lax.dynamic_slice_in_dim(weight, core * half, half, 1)
-    partners = lax.dynamic_slice_in_dim(weight, (1 - core) * half, half, 1)
-    mine, behind = lax.optimization_barrier((mine, behind))
-    mine = [mine] + [shifted(mine, "tp", k) for k in OFFSETS]
-    other = [partners] + [shifted(piece, "sp_1", 1) for piece in mine[1:]]
-    return (mine, other), behind
-
-
-def projected(rows, weights):
-    core = lax.axis_index("sp_1")
-    halves = [
-        sum(jnp.dot(r, w, preferred_element_type=jnp.float32) for r, w in zip(rows, side))
-        for side in weights
-    ]
-    mine, other = halves
-    left, right = jnp.where(core == 0, mine, other), jnp.where(core == 0, other, mine)
-    return jnp.concatenate([left, right], axis=1)
-
-
-def own_rows(rows):
-    count = lax.axis_size("tp")
-    mine = lax.axis_index("tp")
-    blocks = rows.reshape(count, -1, rows.shape[1])
-    parts = [lax.dynamic_index_in_dim(blocks, mine, 0, False)]
-    for k in OFFSETS:
-        block = lax.dynamic_index_in_dim(blocks, (mine + k) % count, 0, False)
-        parts.append(shifted(block, "tp", k))
-    return parts
+    mine = [shifted(mine, "tp", k) for k in OFFSETS]
+    other = [shifted(piece, "sp_1", 1) for piece in mine]
+    return mine, other
 
 
 def split_dot(first, second):
@@ -279,14 +277,20 @@
     )(*arrays)
 
 
-def finish_kernel(core_ref, out_ref, first_ref, reach_ref, gate_ref, gain_ref, gated_ref):
+def finish_kernel(
+    place_ref, out_ref, first_ref, mine_ref, swapped_ref, gate_ref, gain_ref, *refs
+):
+    *blocks, gated_ref = refs
     wide = jnp.float32
     heads = out_ref.shape[0]
-    later_core = core_ref[0] > 0
+    later_core = place_ref[0] > 0
+    mine, swapped = mine_ref[...].astype(wide), swapped_ref[...].astype(wide)
+    low = jnp.where(later_core, swapped, mine)
+    high = jnp.where(later_core, mine, swapped)
     parts = []
     for h in range(heads):
         before = first_ref[h].astype(wide)
-        reach = reach_ref[h]
+        reach = (low, high)[h // 2][:, h % 2 * HEAD : (h % 2 + 1) * HEAD]
         passed = split_dot(before[:, :HEAD], reach) + before[:, HEAD:]
         reach = jnp.where(later_core, passed, reach)
         here = out_ref[h]
@@ -295,19 +299,61 @@
         spread = jnp.mean(centre * centre, axis=1, keepdims=True)
         parts.append(centre * lax.rsqrt(spread + 0.00064))
     normed = jnp.concatenate(parts, axis=1) * gain_ref[...]
-    gated_ref[...] = (normed * jax.nn.sigmoid(gate_ref[...].astype(wide))).astype(gated_ref.dtype)
-
-
-def finished(outputs, first, reach, gate_logits, gain):
-    core = lax.axis_index("sp_1").astype(jnp.int32).reshape(1)
+    gated_ref[...] = normed * jax.nn.sigmoid(gate_ref[...].astype(wide))
+    count = blocks[0].shape[0]
+    for block, k in zip(blocks, (0, *OFFSETS)):
+        start = (place_ref[1] + k) % len(blocks) * count
+        block[...] = gated_ref[pl.ds(pl.multiple_of(start, count), count), :].astype(block.dtype)
+
+
+def finished(outputs, first, mine, swapped, gate_logits, gain):
+    count = lax.axis_size("tp")
+    rows, width = gate_logits.shape
+    place = jnp.stack([lax.axis_index("sp_1"), lax.axis_index("tp")]).astype(jnp.int32)
+    block = jax.ShapeDtypeStruct((rows // count, width), jnp.bfloat16)
     return pl.pallas_call(
         finish_kernel,
-        out_shape=jax.ShapeDtypeStruct(gate_logits.shape, jnp.bfloat16),
-        in_specs=[pl.BlockSpec(memory_space=pltpu.SMEM), *in_vmem(5)],
-        out_specs=in_vmem(1)[0],
+        out_shape=(block,) * count,
+        in_specs=[pl.BlockSpec(memory_space=pltpu.SMEM), *in_vmem(6)],
+        out_specs=tuple(in_vmem(count)),
+        scratch_shapes=[pltpu.VMEM((rows, width), jnp.float32)],
         cost_estimate=pl.CostEstimate(flops=400_000_000, bytes_accessed=1 << 19, transcendentals=0),
+        compiler_params=pltpu.CompilerParams(vmem_limit_bytes=12 << 20),
         name="finish_heads",
-    )(core, outputs, first, reach, gate_logits, gain.reshape(1, -1))
+    )(place, outputs, first, mine, swapped, gate_logits, gain.reshape(1, -1))
+
+
+def project_kernel(count, core_ref, own_ref, weight_ref, *refs):
+    rows, mine, other = refs[:count], refs[count : 2 * count], refs[2 * count : 3 * count]
+    residual_ref, gain_ref, placed_ref, stream_ref, out_ref = refs[3 * count :]
+    halves = []
+    for side in (mine, other):
+        halves.append(sum(plain_dot(r[...], w[...]) for r, w in zip(rows, side)))
+    swap = core_ref[0] > 0
+    left = jnp.where(swap, halves[1], halves[0])
+    right = jnp.where(swap, halves[0], halves[1])
+    branch = plain_dot(own_ref[...], weight_ref[...]) + jnp.concatenate([left, right], axis=1)
+    stream = residual_ref[...].astype(jnp.float32) + branch
+    stream_ref[...] = stream
+    scale = lax.rsqrt(jnp.mean(stream * stream, axis=1, keepdims=True) + 1e-06)
+    normal = (stream * scale * gain_ref[...]).astype(jnp.bfloat16)
+    out_ref[...] = plain_dot(placed_ref[...], normal, ((0,), (0,))).astype(out_ref.dtype)
+
+
+def projected(own, weight, rows, weights, residual, gain, placed):
+    count, width = len(rows), residual.shape[1]
+    return pl.pallas_call(
+        partial(project_kernel, count),
+        out_shape=(
+            jax.ShapeDtypeStruct(residual.shape, jnp.float32),
+            jax.ShapeDtypeStruct((placed.shape[1], width), jnp.bfloat16),
+        ),
+        in_specs=[pl.BlockSpec(memory_space=pltpu.SMEM), *in_vmem(3 * count + 5)],
+        out_specs=tuple(in_vmem(2)),
+        cost_estimate=pl.CostEstimate(flops=800_000_000, bytes_accessed=5 << 20, transcendentals=0),
+        compiler_params=pltpu.CompilerParams(vmem_limit_bytes=20 << 20),
+        name="project_rows",
+    )(core_index(), own, weight, *rows, *weights[0], *weights[1], residual, gain.reshape(1, -1), placed)
 
 
 def hidden_rows(rows, gate, up):
@@ -415,22 +461,14 @@
     outputs, whole = scanned(
         receptance, head_keys, head_values, decay_logits, decay_boost, correction_logits
     )
-    weights, whole = gathered_weight(output_weight, whole)
-    first, reach = incoming_state(whole)
-    gated = finished(outputs, first, reach, gate_logits, head_norm_gain)
-    rows_here = own_rows(gated)
-    branch = projected(rows_here, weights)
-    stream = residual.astype(jnp.float32) + branch
-    normal = (
-        stream
-        * lax.rsqrt(jnp.mean(stream * stream, axis=-1, keepdims=True) + 1e-06)
-        * expert_norm_gain
-    ).astype(jnp.bfloat16)
+    weights = gathered_weight(output_weight)
+    first, mine, swapped = incoming_state(whole)
+    own, *blocks = finished(outputs, first, mine, swapped, gate_logits, head_norm_gain)
+    rows_here = [shifted(b, "tp", k) for b, k in zip(blocks, OFFSETS)]
     sp_count = lax.axis_size(SP)
     tp_count = lax.axis_size("tp")
     capacity = max(2, 2 * TOK_DEV * TOP // (tp_count * sp_count))
-    local_count = normal.shape[0]
-    width_model = normal.shape[1]
+    local_count, width_model = residual.shape
     flat_routes = routes.reshape(-1)
     expert_ids = jnp.arange(sp_count, dtype=jnp.int32)
     chosen = (flat_routes[:, None] == expert_ids[None, :]).astype(jnp.int32)
@@ -441,8 +479,8 @@
     onehot = (place[:, None] == places[None, :]).astype(jnp.bfloat16)
     placed = jnp.sum(onehot.reshape(local_count, TOP, sp_count * capacity), axis=1)
     placed, onehot, routing_weight = lax.optimization_barrier((placed, onehot, routing_weight))
-    outbound = jnp.einsum("ts,td->sd", placed, normal, preferred_element_type=jnp.float32).astype(
-        jnp.bfloat16
+    stream, outbound = projected(
+        own, output_weight, rows_here, weights, residual, expert_norm_gain, placed
     )
     going = outbound.reshape(sp_count, 2 * capacity, width_model // 2)
     arrived = lax.all_to_all(going, SP, split_axis=0, concat_axis=0, tiled=True)

time: 217 us -> 214 us (0.986)
  matrix products: 8.31 us -> 2.13 us
  starting transfers between devices: 52.6 us -> 55.6 us
  other arithmetic: 5.91 us -> 2.95 us
    dot_general x9 -> x0, matrix products: 3.35 us -> none  [the longest x8 3.01 us: projected(): jnp.dot(r, w, preferred_element_type=jnp.float32)]
    ppermute x18, starting transfers between devices: 16.3 us -> 19.3 us  [shifted(): return lax.ppermute(x, axis, [(i, (i + step) % size) for i in range(size)])]
    dot_general x4 -> x3, matrix products: 4.18 us -> 1.35 us  [after(): jnp.einsum('hij,hjk->hik', later[..., :HEAD], earlier, precision=highest)]
  transfers between devices with their start and end apart: 24 -> 24, of which waited for: 13 -> 12; matrix products, arithmetic and copies ran while one was open for 7% -> 2% of each run, Pallas kernels for 6% -> 8%
where the time goes in v1:
time: 214 us; the launch traced here: 213 us
  blocking collectives  80 us (37%)
  starting transfers between devices  55.6 us (26%)
  waiting for transfers between devices  46.8 us (22%)
  Pallas kernels  18.7 us (9%)
  local copies, waits for them, and re-layouts  6.68 us (3%)
  other arithmetic  2.95 us (1%)
    all_to_all x1, blocking collectives, body(): arrived = lax.all_to_all(going, SP, split_axis=0, concat_axis=0, tiled=True)  42.9 us
    ppermute x18, waiting for transfers between devices, shifted(): return lax.ppermute(x, axis, [(i, (i + step) % size) for i in range(size)])  37.8 us
    all_to_all x1, blocking collectives, body(): home = lax.all_to_all(total, SP, split_axis=0, concat_axis=0, tiled=True)  37.1 us
    ppermute x3, starting transfers between devices, across_quads(): lax.ppermute(x, axis, [(i, i + step * QUAD) for i in range(size - step *...  29 us
    ppermute x18, starting transfers between devices, shifted(): return lax.ppermute(x, axis, [(i, (i + step) % size) for i in range(size)])  19.3 us
    ppermute x3, waiting for transfers between devices, within_quads(): return lax.ppermute(x, axis, pairs)  7.64 us
    ppermute x3, starting transfers between devices, within_quads(): return lax.ppermute(x, axis, pairs)  7.32 us
    pallas_call x3, Pallas kernels, more_rows(): pl.pallas_call(partial(more_kernel, len(pieces)), out_shape=jax.ShapeDtyp...  5.43 us
  transfers between devices with their start and end apart: 24, of which 12 were waited for; matrix products, arithmetic and copies ran while one was open for 2% of the time, Pallas kernels for 8%

profile of v1, /device:TPU:40, one launch (start us, length us, event | category | flops | bytes accessed | tf_op | source)
XLA Modules:
  0.0 213.2 jit_solution(13079658257211259097)
XLA Ops:
  0.0 1.9 constant_dynamic-slice_fusion
  1.9 3.3 %collective-permute-start.13 = (bf16[256,1024]{1,0:T(8,128)(2,1)}, bf16[256,1024]{1,0:T(8,128)(2,1)S(1)}, u32[]{:S(2)}, u32[]{:S(2)}) collective-permute-start(bf16[256,1024]{1,0:T(8,128)(2,1)} %constant_dynamic-slice_fusion), channel_id=1, source_target_pairs={{0,2},{1,3},{2,0},{3,1},{4,6},{5,7},{6,4},{7,5},{8,10},{9,11},{10,... | collective-permute-start | bytes 1572872 | tf_op jit(solution)/shard_map/ppermute | solution.py:33
  6.2 1.0 collective-permute-start.11
  7.2 4.1 %scan_blocks.1 = (f32[4,128,128]{2,1,0:T(8,128)}, bf16[4,64,128]{2,1,0:T(8,128)(2,1)}) custom-call(bf16[128,256]{1,0:T(8,128)(2,1)} %query_ref.1, bf16[128,256]{1,0:T(8,128)(2,1)} %key_ref.1, bf16[128,256]{1,0:T(8,128)(2,1)} %value_ref.1, bf16[128,256]{1,0:T(8,128)(2,1)} %decay_ref.1, f32[128,256]{1,0:T(8,128)} %boost_ref.1, bf16[128,256]{1,0:T(8,128)(2,1)} %rate_ref.1), custom_call_target="tpu_custom_call" | custom-call | flops 4000000000 | bytes 1048576 | tf_op jit(solution)/shard_map/scan_blocks/pallas_call | solution.py:267
  14.0 7.3 %collective-permute-start.3 = (bf16[2,64,128]{2,1,0:T(8,128)(2,1)S(1)}, bf16[2,64,128]{2,1,0:T(8,128)(2,1)S(1)}, u32[]{:S(2)}, u32[]{:S(2)}) collective-permute-start(bf16[2,64,128]{2,1,0:T(8,128)(2,1)S(1)} %get-tuple-element.25), channel_id=1, source_target_pairs={{0,24},{8,0},{16,8},{24,16},{32,56},{40,32},{48,40},{56,48},{64,88... | collective-permute-start | bytes 98312 | tf_op jit(solution)/shard_map/ppermute | solution.py:39
  21.3 1.6 collective-permute-done.3
  22.9 3.2 %collective-permute-done.2 = bf16[2,64,128]{2,1,0:T(8,128)(2,1)S(1)} collective-permute-done((bf16[2,64,128]{2,1,0:T(8,128)(2,1)S(1)}, bf16[2,64,128]{2,1,0:T(8,128)(2,1)S(1)}, u32[]{:S(2)}, u32[]{:S(2)}) %collective-permute-start.2) | collective-permute-done | bytes 32800 | tf_op jit(solution)/shard_map/ppermute | solution.py:39
  26.1 2.8 %collective-permute-done.1 = bf16[2,64,128]{2,1,0:T(8,128)(2,1)S(1)} collective-permute-done((bf16[2,64,128]{2,1,0:T(8,128)(2,1)S(1)}, bf16[2,64,128]{2,1,0:T(8,128)(2,1)S(1)}, u32[]{:S(2)}, u32[]{:S(2)}) %collective-permute-start.1) | collective-permute-done | bytes 32800 | tf_op jit(solution)/shard_map/ppermute | solution.py:39
  30.4 20.4 %collective-permute-start.6 = (bf16[2,64,128]{2,1,0:T(8,128)(2,1)S(1)}, bf16[2,64,128]{2,1,0:T(8,128)(2,1)S(1)}, u32[]{:S(2)}, u32[]{:S(2)}) collective-permute-start(bf16[2,64,128]{2,1,0:T(8,128)(2,1)S(1)} %fusion.1), channel_id=1, source_target_pairs={{0,96},{8,104},{16,112},{24,120},{1,97},{9,105},{17,113},{25,121},... | collective-permute-start | bytes 98312 | tf_op jit(solution)/shard_map/ppermute | solution.py:44
  50.8 1.3 collective-permute-start.5
  52.8 7.3 %collective-permute-start.4 = (bf16[2,64,128]{2,1,0:T(8,128)(2,1)S(1)}, bf16[2,64,128]{2,1,0:T(8,128)(2,1)S(1)}, u32[]{:S(2)}, u32[]{:S(2)}) collective-permute-start(bf16[2,64,128]{2,1,0:T(8,128)(2,1)S(1)} %fusion.1), channel_id=1, source_target_pairs={{0,32},{8,40},{16,48},{24,56},{32,64},{40,72},{48,80},{56,88},{64,... | collective-permute-start | bytes 98312 | tf_op jit(solution)/shard_map/ppermute | solution.py:44
  60.3 1.4 collective-permute-done.4
  63.6 2.1 collective-permute-done.7.swapped_ref
  66.7 1.4 finish_heads.1
  69.1 2.5 %collective-permute-start.9 = (bf16[32,256]{1,0:T(8,128)(2,1)S(1)}, bf16[32,256]{1,0:T(8,128)(2,1)S(1)}, u32[]{:S(2)}, u32[]{:S(2)}) collective-permute-start(bf16[32,256]{1,0:T(8,128)(2,1)S(1)} %get-tuple-element.28), channel_id=1, source_target_pairs={{0,3},{1,0},{2,1},{3,2},{4,7},{5,4},{6,5},{7,6},{8,11},{9,8},{10,9... | collective-permute-start | bytes 49160 | tf_op jit(solution)/shard_map/ppermute | solution.py:33
  71.6 1.7 collective-permute-done.8.refs_0_
  73.6 5.0 %collective-permute-done.10.refs_2_ = bf16[32,256]{1,0:T(8,128)(2,1)S(1)} collective-permute-done((bf16[32,256]{1,0:T(8,128)(2,1)S(1)}, bf16[32,256]{1,0:T(8,128)(2,1)S(1)}, u32[]{:S(2)}, u32[]{:S(2)}) %collective-permute-start.10) | collective-permute-done | bytes 16416 | tf_op jit(solution)/shard_map/ppermute | solution.py:33
  78.6 2.4 %project_rows.1 = (f32[32,2048]{1,0:T(8,128)S(1)}, bf16[128,2048]{1,0:T(8,128)(2,1)S(1)}) custom-call(s32[1]{0:T(128)} %bitcast.core_ref, bf16[32,256]{1,0:T(8,128)(2,1)S(1)} %get-tuple-element.26.own_ref, bf16[256,2048]{1,0:T(8,128)(2,1)S(1)} %copy-done, bf16[32,256]{1,0:T(8,128)(2,1)S(1)} %collective-permute-done.8.refs_0_, ...), custom_call_target="tpu_custom_call" | custom-call | flops 800000000 | bytes 5242880 | tf_op jit(solution)/shard_map/project_rows/pallas_call | solution.py:345
  81.8 1.2 reshape.48
  83.1 42.9 %all_to_all.10 = bf16[32,8,1024]{2,1,0:T(8,128)(2,1)S(1)} all-to-all(bf16[32,8,1024]{2,1,0:T(8,128)(2,1)S(1)} %reshape.48), channel_id=1, replica_groups=mesh['grp'=2,'sp_0'=16,'sp_1'=2,'tp'=4] {'sp_0','sp_1'}, dimensions={0} | all-to-all | bytes 1048576 | tf_op jit(solution)/shard_map/all_to_all | solution.py:486
  126.2 1.1 collective-permute-start.19
  127.3 1.0 collective-permute-start.17
  128.3 5.1 %first_rows.1 = (bf16[128,2048]{1,0:T(8,128)(2,1)S(1)}, bf16[2048,896]{1,0:T(8,128)(2,1)S(1)}, bf16[2048,896]{1,0:T(8,128)(2,1)S(1)}, bf16[896,2048]{1,0:T(8,128)(2,1)S(1)}) custom-call(bf16[128,2048]{1,0:T(8,128)(2,1)S(1)} %reshape.49.rows, bf16[2048,896]{1,0:T(8,128)(2,1)} %bitcast.44, bf16[2048,896]{1,0:T(8,128)(2,1)} %bitcast.45, bf16[896,2048]{1,0:T(8,128)(2,1)} %bitcast.46), custom_call_target="tpu_custom_call" | custom-call | flops 1409286144 | bytes 11010048 | tf_op jit(solution)/shard_map/first_rows/pallas_call | solution.py:395
  133.5 6.7 %collective-permute-done.19.refs_0_ = bf16[128,2048]{1,0:T(8,128)(2,1)S(1)} collective-permute-done((bf16[128,2048]{1,0:T(8,128)(2,1)S(1)}, bf16[128,2048]{1,0:T(8,128)(2,1)S(1)}, u32[]{:S(2)}, u32[]{:S(2)}) %collective-permute-start.19) | collective-permute-done | bytes 524320 | tf_op jit(solution)/shard_map/ppermute | solution.py:33
  140.1 2.3 %collective-permute-start.22 = (bf16[64,2048]{1,0:T(8,128)(2,1)S(1)}, bf16[64,2048]{1,0:T(8,128)(2,1)S(1)}, u32[]{:S(2)}, u32[]{:S(2)}) collective-permute-start(bf16[64,2048]{1,0:T(8,128)(2,1)S(1)} %slice.79), channel_id=1, source_target_pairs={{0,3},{1,0},{2,1},{3,2},{4,7},{5,4},{6,5},{7,6},{8,11},{9,8},{10,9... | collective-permute-start | bytes 786440 | tf_op jit(solution)/shard_map/ppermute | solution.py:33
  142.6 1.8 more_rows.3
  144.5 3.5 %collective-permute-start.18 = (bf16[128,2048]{1,0:T(8,128)(2,1)S(1)}, bf16[128,2048]{1,0:T(8,128)(2,1)S(1)}, u32[]{:S(2)}, u32[]{:S(2)}) collective-permute-start(bf16[128,2048]{1,0:T(8,128)(2,1)S(1)} %more_rows.3), channel_id=1, source_target_pairs={{0,3},{1,0},{2,1},{3,2},{4,7},{5,4},{6,5},{7,6},{8,11},{9,8},{10,9... | collective-permute-start | bytes 1572872 | tf_op jit(solution)/shard_map/ppermute | solution.py:33
  148.0 1.8 more_rows.4
  150.9 1.8 more_rows.5
  153.4 16.5 %collective-permute-done.18 = bf16[128,2048]{1,0:T(8,128)(2,1)S(1)} collective-permute-done((bf16[128,2048]{1,0:T(8,128)(2,1)S(1)}, bf16[128,2048]{1,0:T(8,128)(2,1)S(1)}, u32[]{:S(2)}, u32[]{:S(2)}) %collective-permute-start.18) | collective-permute-done | bytes 524320 | tf_op jit(solution)/shard_map/ppermute | solution.py:33
  169.9 4.7 %collective-permute-done.20 = bf16[128,2048]{1,0:T(8,128)(2,1)S(1)} collective-permute-done((bf16[128,2048]{1,0:T(8,128)(2,1)S(1)}, bf16[128,2048]{1,0:T(8,128)(2,1)S(1)}, u32[]{:S(2)}, u32[]{:S(2)}) %collective-permute-start.20) | collective-permute-done | bytes 524320 | tf_op jit(solution)/shard_map/ppermute | solution.py:33
  175.1 37.1 %all_to_all.11 = bf16[32,8,1024]{2,1,0:T(8,128)(2,1)S(1)} all-to-all(bf16[32,8,1024]{2,1,0:T(8,128)(2,1)S(1)} %reshape.50), channel_id=1, replica_groups=mesh['grp'=2,'sp_0'=16,'sp_1'=2,'tp'=4] {'sp_0','sp_1'}, dimensions={0} | all-to-all | bytes 1048576 | tf_op jit(solution)/shard_map/all_to_all | solution.py:501
  (85 shorter events, 14.5 us)
Async XLA Ops:
  1.9 9.6 %copy-start.9 = (s32[32,2]{0,1:T(2,128)S(1)}, s32[32,2]{0,1:T(2,128)}, u32[]{:S(2)}) copy-start(s32[32,2]{0,1:T(2,128)} %param.27) | copy-start | bytes 772
  1.9 60.1 %collective-permute-start.13 = (bf16[256,1024]{1,0:T(8,128)(2,1)}, bf16[256,1024]{1,0:T(8,128)(2,1)S(1)}, u32[]{:S(2)}, u32[]{:S(2)}) collective-permute-start(bf16[256,1024]{1,0:T(8,128)(2,1)} %constant_dynamic-slice_fusion), channel_id=1, source_target_pairs={{0,2},{1,3},{2,0},{3,1},{4,6},{5,7},{6,4},{7,5},{8,10},{9,11},{10,... | collective-permute-start | bytes 1572872 | tf_op jit(solution)/shard_map/ppermute | solution.py:33
  5.2 57.0 %collective-permute-start.12 = (bf16[256,1024]{1,0:T(8,128)(2,1)}, bf16[256,1024]{1,0:T(8,128)(2,1)S(1)}, u32[]{:S(2)}, u32[]{:S(2)}) collective-permute-start(bf16[256,1024]{1,0:T(8,128)(2,1)} %constant_dynamic-slice_fusion), channel_id=1, source_target_pairs={{0,3},{1,0},{2,1},{3,2},{4,7},{5,4},{6,5},{7,6},{8,11},{9,8},{10,9... | collective-permute-start | bytes 1572872 | tf_op jit(solution)/shard_map/ppermute | solution.py:33
  6.2 56.5 %collective-permute-start.11 = (bf16[256,1024]{1,0:T(8,128)(2,1)}, bf16[256,1024]{1,0:T(8,128)(2,1)S(1)}, u32[]{:S(2)}, u32[]{:S(2)}) collective-permute-start(bf16[256,1024]{1,0:T(8,128)(2,1)} %constant_dynamic-slice_fusion), channel_id=1, source_target_pairs={{0,1},{1,2},{2,3},{3,0},{4,5},{5,6},{6,7},{7,4},{8,9},{9,10},{10,1... | collective-permute-start | bytes 1572872 | tf_op jit(solution)/shard_map/ppermute | solution.py:33
  7.2 58.5 %copy-start.6 = (f32[256]{0:T(256)S(1)}, f32[256]{0:T(256)}, u32[]{:S(2)}) copy-start(f32[256]{0:T(256)} %param.23) | copy-start | bytes 3076
  11.3 54.4 %copy-start.4 = (bf16[128,256]{1,0:T(8,128)(2,1)S(1)}, bf16[128,256]{1,0:T(8,128)(2,1)}, u32[]{:S(2)}) copy-start(bf16[128,256]{1,0:T(8,128)(2,1)} %gate_ref.1) | copy-start | bytes 196612
  11.3 67.3 %copy-start = (bf16[256,2048]{1,0:T(8,128)(2,1)S(1)}, bf16[256,2048]{1,0:T(8,128)(2,1)}, u32[]{:S(2)}) copy-start(bf16[256,2048]{1,0:T(8,128)(2,1)} %weight_ref.1) | copy-start | bytes 3145732
  11.3 67.3 %copy-start.2 = (bf16[32,2048]{1,0:T(8,128)(2,1)S(1)}, bf16[32,2048]{1,0:T(8,128)(2,1)}, u32[]{:S(2)}) copy-start(bf16[32,2048]{1,0:T(8,128)(2,1)} %refs_9_.1) | copy-start | bytes 393220
  11.3 67.3 %copy-start.3 = (f32[2048]{0:T(1024)S(1)}, f32[2048]{0:T(1024)}, u32[]{:S(2)}) copy-start(f32[2048]{0:T(1024)} %param.26) | copy-start | bytes 24580
  11.4 1.6 collective-permute-start
  14.0 8.9 %collective-permute-start.3 = (bf16[2,64,128]{2,1,0:T(8,128)(2,1)S(1)}, bf16[2,64,128]{2,1,0:T(8,128)(2,1)S(1)}, u32[]{:S(2)}, u32[]{:S(2)}) collective-permute-start(bf16[2,64,128]{2,1,0:T(8,128)(2,1)S(1)} %get-tuple-element.25), channel_id=1, source_target_pairs={{0,24},{8,0},{16,8},{24,16},{32,56},{40,32},{48,40},{56,48},{64,88... | collective-permute-start | bytes 98312 | tf_op jit(solution)/shard_map/ppermute | solution.py:39
  21.3 4.8 %collective-permute-start.2 = (bf16[2,64,128]{2,1,0:T(8,128)(2,1)S(1)}, bf16[2,64,128]{2,1,0:T(8,128)(2,1)S(1)}, u32[]{:S(2)}, u32[]{:S(2)}) collective-permute-start(bf16[2,64,128]{2,1,0:T(8,128)(2,1)S(1)} %get-tuple-element.25), channel_id=1, source_target_pairs={{0,16},{8,24},{16,0},{24,8},{32,48},{40,56},{48,32},{56,40},{64,80... | collective-permute-start | bytes 98312 | tf_op jit(solution)/shard_map/ppermute | solution.py:39
  22.9 6.1 %collective-permute-start.1 = (bf16[2,64,128]{2,1,0:T(8,128)(2,1)S(1)}, bf16[2,64,128]{2,1,0:T(8,128)(2,1)S(1)}, u32[]{:S(2)}, u32[]{:S(2)}) collective-permute-start(bf16[2,64,128]{2,1,0:T(8,128)(2,1)S(1)} %get-tuple-element.25), channel_id=1, source_target_pairs={{0,8},{8,16},{16,24},{24,0},{32,40},{40,48},{48,56},{56,32},{64,72... | collective-permute-start | bytes 98312 | tf_op jit(solution)/shard_map/ppermute | solution.py:39
  30.4 22.4 %collective-permute-start.6 = (bf16[2,64,128]{2,1,0:T(8,128)(2,1)S(1)}, bf16[2,64,128]{2,1,0:T(8,128)(2,1)S(1)}, u32[]{:S(2)}, u32[]{:S(2)}) collective-permute-start(bf16[2,64,128]{2,1,0:T(8,128)(2,1)S(1)} %fusion.1), channel_id=1, source_target_pairs={{0,96},{8,104},{16,112},{24,120},{1,97},{9,105},{17,113},{25,121},... | collective-permute-start | bytes 98312 | tf_op jit(solution)/shard_map/ppermute | solution.py:44
  50.8 9.3 %collective-permute-start.5 = (bf16[2,64,128]{2,1,0:T(8,128)(2,1)S(1)}, bf16[2,64,128]{2,1,0:T(8,128)(2,1)S(1)}, u32[]{:S(2)}, u32[]{:S(2)}) collective-permute-start(bf16[2,64,128]{2,1,0:T(8,128)(2,1)S(1)} %fusion.1), channel_id=1, source_target_pairs={{0,64},{8,72},{16,80},{24,88},{32,96},{40,104},{48,112},{56,120},{... | collective-permute-start | bytes 98312 | tf_op jit(solution)/shard_map/ppermute | solution.py:44
  52.8 8.9 %collective-permute-start.4 = (bf16[2,64,128]{2,1,0:T(8,128)(2,1)S(1)}, bf16[2,64,128]{2,1,0:T(8,128)(2,1)S(1)}, u32[]{:S(2)}, u32[]{:S(2)}) collective-permute-start(bf16[2,64,128]{2,1,0:T(8,128)(2,1)S(1)} %fusion.1), channel_id=1, source_target_pairs={{0,32},{8,40},{16,48},{24,56},{32,64},{40,72},{48,80},{56,88},{64,... | collective-permute-start | bytes 98312 | tf_op jit(solution)/shard_map/ppermute | solution.py:44
  62.0 16.5 %collective-permute-start.16 = (bf16[256,1024]{1,0:T(8,128)(2,1)S(1)}, bf16[256,1024]{1,0:T(8,128)(2,1)S(1)}, u32[]{:S(2)}, u32[]{:S(2)}) collective-permute-start(bf16[256,1024]{1,0:T(8,128)(2,1)S(1)} %collective-permute-done.13.refs_5_), channel_id=1, source_target_pairs={{0,4},{4,0},{1,5},{5,1},{2,6},{6,2},{3,7},{7,3},{8,12},{12,8},{9,1... | collective-permute-start | bytes 1572872 | tf_op jit(solution)/shard_map/ppermute | solution.py:33
  62.2 16.4 %collective-permute-start.15 = (bf16[256,1024]{1,0:T(8,128)(2,1)S(1)}, bf16[256,1024]{1,0:T(8,128)(2,1)}, u32[]{:S(2)}, u32[]{:S(2)}) collective-permute-start(bf16[256,1024]{1,0:T(8,128)(2,1)S(1)} %collective-permute-done.12.refs_4_), channel_id=1, source_target_pairs={{0,4},{4,0},{1,5},{5,1},{2,6},{6,2},{3,7},{7,3},{8,12},{12,8},{9,1... | collective-permute-start | bytes 1572872 | tf_op jit(solution)/shard_map/ppermute | solution.py:33
  62.7 15.9 %collective-permute-start.14 = (bf16[256,1024]{1,0:T(8,128)(2,1)S(1)}, bf16[256,1024]{1,0:T(8,128)(2,1)}, u32[]{:S(2)}, u32[]{:S(2)}) collective-permute-start(bf16[256,1024]{1,0:T(8,128)(2,1)S(1)} %collective-permute-done.11.refs_3_), channel_id=1, source_target_pairs={{0,4},{4,0},{1,5},{5,1},{2,6},{6,2},{3,7},{7,3},{8,12},{12,8},{9,1... | collective-permute-start | bytes 1572872 | tf_op jit(solution)/shard_map/ppermute | solution.py:33
  62.9 2.8 %collective-permute-start.7 = (bf16[64,128]{1,0:T(8,128)(2,1)S(1)}, bf16[64,128]{1,0:T(8,128)(2,1)S(1)}, u32[]{:S(2)}, u32[]{:S(2)}) collective-permute-start(bf16[64,128]{1,0:T(8,128)(2,1)S(1)} %pad_maximum_fusion.1.mine_ref), channel_id=1, source_target_pairs={{0,4},{4,0},{1,5},{5,1},{2,6},{6,2},{3,7},{7,3},{8,12},{12,8},{9,1... | collective-permute-start | bytes 49160 | tf_op jit(solution)/shard_map/ppermute | solution.py:33
  68.1 5.2 %collective-permute-start.8 = (bf16[32,256]{1,0:T(8,128)(2,1)S(1)}, bf16[32,256]{1,0:T(8,128)(2,1)S(1)}, u32[]{:S(2)}, u32[]{:S(2)}) collective-permute-start(bf16[32,256]{1,0:T(8,128)(2,1)S(1)} %get-tuple-element.27), channel_id=1, source_target_pairs={{0,1},{1,2},{2,3},{3,0},{4,5},{5,6},{6,7},{7,4},{8,9},{9,10},{10,1... | collective-permute-start | bytes 49160 | tf_op jit(solution)/shard_map/ppermute | solution.py:33
  69.1 4.5 %collective-permute-start.9 = (bf16[32,256]{1,0:T(8,128)(2,1)S(1)}, bf16[32,256]{1,0:T(8,128)(2,1)S(1)}, u32[]{:S(2)}, u32[]{:S(2)}) collective-permute-start(bf16[32,256]{1,0:T(8,128)(2,1)S(1)} %get-tuple-element.28), channel_id=1, source_target_pairs={{0,3},{1,0},{2,1},{3,2},{4,7},{5,4},{6,5},{7,6},{8,11},{9,8},{10,9... | collective-permute-start | bytes 49160 | tf_op jit(solution)/shard_map/ppermute | solution.py:33
  73.3 5.2 %collective-permute-start.10 = (bf16[32,256]{1,0:T(8,128)(2,1)S(1)}, bf16[32,256]{1,0:T(8,128)(2,1)S(1)}, u32[]{:S(2)}, u32[]{:S(2)}) collective-permute-start(bf16[32,256]{1,0:T(8,128)(2,1)S(1)} %get-tuple-element.29), channel_id=1, source_target_pairs={{0,2},{1,3},{2,0},{3,1},{4,6},{5,7},{6,4},{7,5},{8,10},{9,11},{10,... | collective-permute-start | bytes 49160 | tf_op jit(solution)/shard_map/ppermute | solution.py:33
  126.2 13.9 %collective-permute-start.19 = (bf16[128,2048]{1,0:T(8,128)(2,1)S(1)}, bf16[128,2048]{1,0:T(8,128)(2,1)S(1)}, u32[]{:S(2)}, u32[]{:S(2)}) collective-permute-start(bf16[128,2048]{1,0:T(8,128)(2,1)S(1)} %reshape.49.rows), channel_id=1, source_target_pairs={{0,3},{1,0},{2,1},{3,2},{4,7},{5,4},{6,5},{7,6},{8,11},{9,8},{10,9... | collective-permute-start | bytes 1572872 | tf_op jit(solution)/shard_map/ppermute | solution.py:33
  127.3 15.2 %collective-permute-start.17 = (bf16[128,2048]{1,0:T(8,128)(2,1)S(1)}, bf16[128,2048]{1,0:T(8,128)(2,1)S(1)}, u32[]{:S(2)}, u32[]{:S(2)}) collective-permute-start(bf16[128,2048]{1,0:T(8,128)(2,1)S(1)} %reshape.49.rows), channel_id=1, source_target_pairs={{0,1},{1,2},{2,3},{3,0},{4,5},{5,6},{6,7},{7,4},{8,9},{9,10},{10,1... | collective-permute-start | bytes 1572872 | tf_op jit(solution)/shard_map/ppermute | solution.py:33
  140.1 9.8 %collective-permute-start.22 = (bf16[64,2048]{1,0:T(8,128)(2,1)S(1)}, bf16[64,2048]{1,0:T(8,128)(2,1)S(1)}, u32[]{:S(2)}, u32[]{:S(2)}) collective-permute-start(bf16[64,2048]{1,0:T(8,128)(2,1)S(1)} %slice.79), channel_id=1, source_target_pairs={{0,3},{1,0},{2,1},{3,2},{4,7},{5,4},{6,5},{7,6},{8,11},{9,8},{10,9... | collective-permute-start | bytes 786440 | tf_op jit(solution)/shard_map/ppermute | solution.py:33
  142.5 8.4 %collective-permute-start.21 = (bf16[64,2048]{1,0:T(8,128)(2,1)S(1)}, bf16[64,2048]{1,0:T(8,128)(2,1)S(1)}, u32[]{:S(2)}, u32[]{:S(2)}) collective-permute-start(bf16[64,2048]{1,0:T(8,128)(2,1)S(1)} %slice.78), channel_id=1, source_target_pairs={{0,1},{1,2},{2,3},{3,0},{4,5},{5,6},{6,7},{7,4},{8,9},{9,10},{10,1... | collective-permute-start | bytes 786440 | tf_op jit(solution)/shard_map/ppermute | solution.py:33
  144.5 25.4 %collective-permute-start.18 = (bf16[128,2048]{1,0:T(8,128)(2,1)S(1)}, bf16[128,2048]{1,0:T(8,128)(2,1)S(1)}, u32[]{:S(2)}, u32[]{:S(2)}) collective-permute-start(bf16[128,2048]{1,0:T(8,128)(2,1)S(1)} %more_rows.3), channel_id=1, source_target_pairs={{0,3},{1,0},{2,1},{3,2},{4,7},{5,4},{6,5},{7,6},{8,11},{9,8},{10,9... | collective-permute-start | bytes 1572872 | tf_op jit(solution)/shard_map/ppermute | solution.py:33
  149.8 24.7 %collective-permute-start.20 = (bf16[128,2048]{1,0:T(8,128)(2,1)S(1)}, bf16[128,2048]{1,0:T(8,128)(2,1)S(1)}, u32[]{:S(2)}, u32[]{:S(2)}) collective-permute-start(bf16[128,2048]{1,0:T(8,128)(2,1)S(1)} %more_rows.4), channel_id=1, source_target_pairs={{0,1},{1,2},{2,3},{3,0},{4,5},{5,6},{6,7},{7,4},{8,9},{9,10},{10,1... | collective-permute-start | bytes 1572872 | tf_op jit(solution)/shard_map/ppermute | solution.py:33
  152.7 59.6 %copy-start.8 = (bf16[64,128]{1,0:T(8,128)(2,1)S(1)}, bf16[64,128]{1,0:T(8,128)(2,1)}, u32[]{:S(2)}) copy-start(bf16[64,128]{1,0:T(8,128)(2,1)} %fusion.17) | copy-start | bytes 49156
  152.7 59.6 %copy-start.10 = (f32[32,2]{0,1:T(2,128)S(1)}, f32[32,2]{0,1:T(2,128)}, u32[]{:S(2)}) copy-start(f32[32,2]{0,1:T(2,128)} %param.28) | copy-start | bytes 772
  152.8 21.8 %collective-permute-start.23 = (bf16[128,2048]{1,0:T(8,128)(2,1)S(1)}, bf16[128,2048]{1,0:T(8,128)(2,1)S(1)}, u32[]{:S(2)}, u32[]{:S(2)}) collective-permute-start(bf16[128,2048]{1,0:T(8,128)(2,1)S(1)} %more_rows.5), channel_id=1, source_target_pairs={{0,2},{1,3},{2,0},{3,1},{4,6},{5,7},{6,4},{7,5},{8,10},{9,11},{10,... | collective-permute-start | bytes 1572872 | tf_op jit(solution)/shard_map/ppermute | solution.py:33
  (3 other events, 2.6 us)

commit v2 on v1

--- a/solution.py
+++ b/solution.py
@@ -25,9 +25,6 @@
 GRP_SP_TP = ("grp", "sp_0", "sp_1", "tp")
 
 
-highest = lax.Precision.HIGHEST
-
-
 def shifted(x, axis, step):
     size = lax.axis_size(axis)
     return lax.ppermute(x, axis, [(i, (i + step) % size) for i in range(size)])
@@ -42,16 +39,6 @@
 def across_quads(x, axis, step):
     size = lax.axis_size(axis)
     return lax.ppermute(x, axis, [(i, i + step * QUAD) for i in range(size - step * QUAD)])
-
-
-def after(later, earlier):
-    moved = jnp.einsum("hij,hjk->hik", later[..., :HEAD], earlier, precision=highest)
-    return moved + jnp.where(jnp.arange(2 * HEAD) < HEAD, 0.0, later)
-
-
-def onto(later, state):
-    moved = jnp.einsum("hij,hjk->hik", later[..., :HEAD], state, precision=highest)
-    return moved + later[..., HEAD:]
 
 
 def chip_kernel(core_ref, own_ref, other_ref, chip_ref, sent_ref):
@@ -62,8 +49,7 @@
         other = other_ref[core * half + h].astype(jnp.float32)
         first = jnp.where(core == 0, own, other)
         second = jnp.where(core == 0, other, own)
-        state = lax.broadcasted_iota(jnp.int32, second.shape, 1) >= HEAD
-        chip = split_dot(second[:, :HEAD], first) + jnp.where(state, second, 0.0)
+        chip = joined(second, first)
         chip_ref[h] = chip
         sent_ref[h] = chip.astype(sent_ref.dtype)
 
@@ -88,28 +74,81 @@
     )(core_index(), own, other)
 
 
+def joined(later, earlier):
+    state = lax.broadcasted_iota(jnp.int32, later.shape, 1) >= HEAD
+    return split_dot(later[:, :HEAD], earlier) + jnp.where(state, later, 0.0)
+
+
+def quad_kernel(member_ref, chip_ref, *refs):
+    *came, before_ref, sent_ref = refs
+    member = member_ref[0]
+    for h in range(chip_ref.shape[0]):
+        pieces = [chip_ref[h]] + [piece[h].astype(jnp.float32) for piece in came]
+        ordered = []
+        for place in range(QUAD):
+            piece = pieces[0]
+            for k in range(1, QUAD):
+                piece = jnp.where(member == (place + k) % QUAD, pieces[k], piece)
+            ordered.append(piece)
+        total = ordered[0]
+        row = lax.broadcasted_iota(jnp.int32, total.shape, 0)
+        col = lax.broadcasted_iota(jnp.int32, total.shape, 1)
+        before = jnp.where(member == 0, (row == col).astype(jnp.float32), total)
+        for place in range(1, QUAD):
+            total = joined(ordered[place], total)
+            if place < QUAD - 1:
+                before = jnp.where(member == place + 1, total, before)
+        before_ref[h] = before
+        sent_ref[h] = total.astype(sent_ref.dtype)
+
+
+def quad_map(chip, came):
+    member = (lax.axis_index("sp_0") % QUAD).astype(jnp.int32).reshape(1)
+    return pl.pallas_call(
+        quad_kernel,
+        out_shape=(
+            jax.ShapeDtypeStruct(chip.shape, jnp.float32),
+            jax.ShapeDtypeStruct(chip.shape, jnp.bfloat16),
+        ),
+        in_specs=[pl.BlockSpec(memory_space=pltpu.SMEM), *in_vmem(QUAD)],
+        out_specs=tuple(in_vmem(2)),
+        compiler_params=pltpu.CompilerParams(vmem_limit_bytes=8 << 20),
+        cost_estimate=pl.CostEstimate(flops=200_000_000, bytes_accessed=1 << 18, transcendentals=0),
+        name="quad_map",
+    )(member, chip, *came)
+
+
+def far_kernel(before_ref, *refs):
+    *far, mine_ref = refs
+    wide = jnp.float32
+    for h in range(before_ref.shape[0]):
+        reach = far[0][h][:, HEAD:].astype(wide)
+        for piece in [*far[1:], before_ref]:
+            later = piece[h].astype(wide)
+            reach = split_dot(later[:, :HEAD], reach) + later[:, HEAD:]
+        mine_ref[:, h * HEAD : (h + 1) * HEAD] = reach.astype(mine_ref.dtype)
+
+
+def far_state(before, far):
+    heads = before.shape[0]
+    return pl.pallas_call(
+        far_kernel,
+        out_shape=jax.ShapeDtypeStruct((HEAD, heads * HEAD), jnp.bfloat16),
+        in_specs=in_vmem(QUAD),
+        out_specs=in_vmem(1)[0],
+        compiler_params=pltpu.CompilerParams(vmem_limit_bytes=8 << 20),
+        cost_estimate=pl.CostEstimate(flops=200_000_000, bytes_accessed=1 << 18, transcendentals=0),
+        name="far_state",
+    )(before, *far)
+
+
 def incoming_state(packed):
-    wide = jnp.float32
     other = shifted(packed, "sp_1", 1)
     chip, sent = chip_map(packed, other)
-    member = lax.axis_index("sp_0") % QUAD
-    came = [chip] + [within_quads(sent, "sp_0", k).astype(wide) for k in range(1, QUAD)]
-    came = jnp.stack(came)
-    total = lax.dynamic_index_in_dim(came, member % QUAD, 0, False)
-    eye = jnp.eye(HEAD, 2 * HEAD, dtype=wide)
-    before = jnp.where(member == 0, eye, total)
-    for k in range(1, QUAD):
-        piece = lax.dynamic_index_in_dim(came, (member - k) % QUAD, 0, False)
-        total = after(piece, total)
-        if k < QUAD - 1:
-            before = jnp.where(member == k + 1, total, before)
-    sent = total.astype(jnp.bfloat16)
-    far = [across_quads(sent, "sp_0", k).astype(wide) for k in range(QUAD - 1, 0, -1)]
-    reach = far[0][..., HEAD:]
-    for piece in far[1:]:
-        reach = onto(piece, reach)
-    reach = onto(before, reach)
-    mine = jnp.concatenate([reach[0], reach[1]], axis=1).astype(jnp.bfloat16)
+    came = [within_quads(sent, "sp_0", k) for k in range(1, QUAD)]
+    before, sent = quad_map(chip, came)
+    far = [across_quads(sent, "sp_0", k) for k in range(QUAD - 1, 0, -1)]
+    mine = far_state(before, far)
     swapped = shifted(mine, "sp_1", 1)
     return other, mine, swapped
 
@@ -323,9 +362,9 @@
     )(place, outputs, first, mine, swapped, gate_logits, gain.reshape(1, -1))
 
 
-def project_kernel(count, core_ref, own_ref, weight_ref, *refs):
+def project_kernel(count, capacity, core_ref, own_ref, weight_ref, *refs):
     rows, mine, other = refs[:count], refs[count : 2 * count], refs[2 * count : 3 * count]
-    residual_ref, gain_ref, placed_ref, stream_ref, out_ref = refs[3 * count :]
+    residual_ref, gain_ref, column_ref, line_ref, stream_ref, out_ref, onehot_ref = refs[3 * count :]
     halves = []
     for side in (mine, other):
         halves.append(sum(plain_dot(r[...], w[...]) for r, w in zip(rows, side)))
@@ -337,23 +376,56 @@
     stream_ref[...] = stream
     scale = lax.rsqrt(jnp.mean(stream * stream, axis=1, keepdims=True) + 1e-06)
     normal = (stream * scale * gain_ref[...]).astype(jnp.bfloat16)
-    out_ref[...] = plain_dot(placed_ref[...], normal, ((0,), (0,))).astype(out_ref.dtype)
-
-
-def projected(own, weight, rows, weights, residual, gain, placed):
+    tokens, total = stream.shape[0], line_ref.shape[1]
+    expert = column_ref[...]
+    row = lax.broadcasted_iota(jnp.int32, (total, total), 0)
+    col = lax.broadcasted_iota(jnp.int32, (total, total), 1)
+    earlier = (expert == line_ref[...]) & (col < row)
+    rank = jnp.sum(earlier.astype(jnp.float32), axis=1, keepdims=True).astype(jnp.int32)
+    slot = lax.broadcasted_iota(jnp.int32, onehot_ref.shape, 1)
+    onehot = (expert * capacity + rank == slot).astype(jnp.float32)
+    onehot_ref[...] = onehot.astype(onehot_ref.dtype)
+    placed = sum(onehot[k : k + tokens] for k in range(0, total, tokens))
+    out_ref[...] = plain_dot(placed, normal, ((0,), (0,))).astype(out_ref.dtype)
+
+
+def projected(own, weight, rows, weights, residual, gain, routes, experts, capacity):
     count, width = len(rows), residual.shape[1]
-    return pl.pallas_call(
-        partial(project_kernel, count),
+    flat = routes.T.reshape(-1)
+    return pl.pallas_call(
+        partial(project_kernel, count, capacity),
         out_shape=(
             jax.ShapeDtypeStruct(residual.shape, jnp.float32),
-            jax.ShapeDtypeStruct((placed.shape[1], width), jnp.bfloat16),
+            jax.ShapeDtypeStruct((experts * capacity, width), jnp.bfloat16),
+            jax.ShapeDtypeStruct((routes.size, experts * capacity), jnp.bfloat16),
         ),
-        in_specs=[pl.BlockSpec(memory_space=pltpu.SMEM), *in_vmem(3 * count + 5)],
-        out_specs=tuple(in_vmem(2)),
+        in_specs=[pl.BlockSpec(memory_space=pltpu.SMEM), *in_vmem(3 * count + 6)],
+        out_specs=tuple(in_vmem(3)),
         cost_estimate=pl.CostEstimate(flops=800_000_000, bytes_accessed=5 << 20, transcendentals=0),
         compiler_params=pltpu.CompilerParams(vmem_limit_bytes=20 << 20),
         name="project_rows",
-    )(core_index(), own, weight, *rows, *weights[0], *weights[1], residual, gain.reshape(1, -1), placed)
+    )(core_index(), own, weight, *rows, *weights[0], *weights[1], residual, gain.reshape(1, -1), flat.reshape(-1, 1), flat.reshape(1, -1))
+
+
+def combine_kernel(onehot_ref, weight_ref, stream_ref, home_ref, out_ref):
+    tokens = stream_ref.shape[0]
+    picked = plain_dot(onehot_ref[...], home_ref[...])
+    total = stream_ref[...]
+    for k in range(weight_ref.shape[1]):
+        total = total + picked[k * tokens : (k + 1) * tokens] * weight_ref[:, k : k + 1]
+    out_ref[...] = total.astype(out_ref.dtype)
+
+
+def combined(onehot, weight, stream, home):
+    return pl.pallas_call(
+        combine_kernel,
+        out_shape=jax.ShapeDtypeStruct(stream.shape, jnp.bfloat16),
+        in_specs=in_vmem(4),
+        out_specs=in_vmem(1)[0],
+        compiler_params=pltpu.CompilerParams(vmem_limit_bytes=12 << 20),
+        cost_estimate=pl.CostEstimate(flops=100_000_000, bytes_accessed=1 << 20, transcendentals=0),
+        name="combine_rows",
+    )(onehot, weight, stream, home)
 
 
 def hidden_rows(rows, gate, up):
@@ -468,19 +540,17 @@
     sp_count = lax.axis_size(SP)
     tp_count = lax.axis_size("tp")
     capacity = max(2, 2 * TOK_DEV * TOP // (tp_count * sp_count))
-    local_count, width_model = residual.shape
-    flat_routes = routes.reshape(-1)
-    expert_ids = jnp.arange(sp_count, dtype=jnp.int32)
-    chosen = (flat_routes[:, None] == expert_ids[None, :]).astype(jnp.int32)
-    earlier = jnp.cumsum(chosen, axis=0) - chosen
-    rank = jnp.sum(earlier * chosen, axis=1)
-    place = flat_routes * capacity + rank
-    places = jnp.arange(sp_count * capacity, dtype=jnp.int32)
-    onehot = (place[:, None] == places[None, :]).astype(jnp.bfloat16)
-    placed = jnp.sum(onehot.reshape(local_count, TOP, sp_count * capacity), axis=1)
-    placed, onehot, routing_weight = lax.optimization_barrier((placed, onehot, routing_weight))
-    stream, outbound = projected(
-        own, output_weight, rows_here, weights, residual, expert_norm_gain, placed
+    width_model = residual.shape[1]
+    stream, outbound, onehot = projected(
+        own,
+        output_weight,
+        rows_here,
+        weights,
+        residual,
+        expert_norm_gain,
+        routes,
+        sp_count,
+        capacity,
     )
     going = outbound.reshape(sp_count, 2 * capacity, width_model // 2)
     arrived = lax.all_to_all(going, SP, split_axis=0, concat_axis=0, tiled=True)
@@ -500,11 +570,7 @@
     total = total.reshape(sp_count, 2 * capacity, width_model // 2)
     home = lax.all_to_all(total, SP, split_axis=0, concat_axis=0, tiled=True)
     home = home.reshape(-1, width_model)
-    picked = jnp.dot(onehot, home, preferred_element_type=jnp.float32)
-    routed = jnp.sum(
-        picked.reshape(local_count, TOP, width_model) * routing_weight[:, :, None], axis=1
-    )
-    return (stream + routed).astype(jnp.bfloat16)
+    return combined(onehot, routing_weight, stream, home)
 
 
 def solution(mesh):

time: 214 us -> 239 us (1.12)
  waiting for transfers between devices: 46.8 us -> 101 us
  blocking collectives: 80 us -> 43.9 us
  starting transfers between devices: 55.6 us -> 62.2 us
  other arithmetic: 2.95 us -> 0.41 us
    all_to_all x1 -> x0, blocking collectives: 37.1 us -> none  [body(): home = lax.all_to_all(total, SP, split_axis=0, concat_axis=0, tiled=True)]
    all_to_all x0 -> x1, waiting for transfers between devices: none -> 33.1 us  [body(): home = lax.all_to_all(total, SP, split_axis=0, concat_axis=0, tiled=True)]
    ppermute x18, waiting for transfers between devices: 37.8 us -> 58.5 us  [shifted(): return lax.ppermute(x, axis, [(i, (i + step) % size) for i in range(size)])]
    all_to_all x0 -> x1, starting transfers between devices: none -> 4.8 us  [body(): home = lax.all_to_all(total, SP, split_axis=0, concat_axis=0, tiled=True)]
    unnamed x23 -> x25, local copies, waits for them, and re-layouts: 2.72 us -> 5.05 us
  transfers between devices with their start and end apart: 24 -> 25, of which waited for: 12 -> 15; matrix products, arithmetic and copies ran while one was open for 2% -> 0% of each run, Pallas kernels for 8% -> 7%
where the time goes in v2:
time: 239 us; the launch traced here: 237 us
  waiting for transfers between devices  101 us (42%)
  starting transfers between devices  62.2 us (26%)
  blocking collectives  43.9 us (18%)
  Pallas kernels  20.9 us (9%)
  local copies, waits for them, and re-layouts  8.86 us (4%)
    ppermute x18, waiting for transfers between devices, shifted(): return lax.ppermute(x, axis, [(i, (i + step) % size) for i in range(size)])  58.5 us
    all_to_all x1, blocking collectives, body(): arrived = lax.all_to_all(going, SP, split_axis=0, concat_axis=0, tiled=True)  43.9 us
    all_to_all x1, waiting for transfers between devices, body(): home = lax.all_to_all(total, SP, split_axis=0, concat_axis=0, tiled=True)  33.1 us
    ppermute x3, starting transfers between devices, across_quads(): lax.ppermute(x, axis, [(i, i + step * QUAD) for i in range(size - step *...  30.1 us
    ppermute x18, starting transfers between devices, shifted(): return lax.ppermute(x, axis, [(i, (i + step) % size) for i in range(size)])  20.1 us
    ppermute x3, waiting for transfers between devices, within_quads(): return lax.ppermute(x, axis, pairs)  7.73 us
    ppermute x3, starting transfers between devices, within_quads(): return lax.ppermute(x, axis, pairs)  7.21 us
    pallas_call x3, Pallas kernels, more_rows(): pl.pallas_call(partial(more_kernel, len(pieces)), out_shape=jax.ShapeDtyp...  5.44 us
  transfers between devices with their start and end apart: 25, of which 15 were waited for; matrix products, arithmetic and copies ran while one was open for 0% of the time, Pallas kernels for 7%

profile of v2, /device:TPU:40, one launch (start us, length us, event | category | flops | bytes accessed | tf_op | source)
XLA Modules:
  0.0 237.4 jit_solution(12155926101112045763)
XLA Ops:
  1.1 3.4 %collective-permute-start.13 = (bf16[256,1024]{1,0:T(8,128)(2,1)S(1)}, bf16[256,1024]{1,0:T(8,128)(2,1)S(1)}, u32[]{:S(2)}, u32[]{:S(2)}) collective-permute-start(bf16[256,1024]{1,0:T(8,128)(2,1)S(1)} %constant_dynamic-slice_fusion), channel_id=1, source_target_pairs={{0,2},{1,3},{2,0},{3,1},{4,6},{5,7},{6,4},{7,5},{8,10},{9,11},{10,... | collective-permute-start | bytes 1572872 | tf_op jit(solution)/shard_map/ppermute | solution.py:30
  6.5 11.0 %collective-permute-done.13.refs_5_ = bf16[256,1024]{1,0:T(8,128)(2,1)S(1)} collective-permute-done((bf16[256,1024]{1,0:T(8,128)(2,1)S(1)}, bf16[256,1024]{1,0:T(8,128)(2,1)S(1)}, u32[]{:S(2)}, u32[]{:S(2)}) %collective-permute-start.13) | collective-permute-done | bytes 524320 | tf_op jit(solution)/shard_map/ppermute | solution.py:30
  17.6 10.7 %collective-permute-done.12.refs_4_ = bf16[256,1024]{1,0:T(8,128)(2,1)S(1)} collective-permute-done((bf16[256,1024]{1,0:T(8,128)(2,1)S(1)}, bf16[256,1024]{1,0:T(8,128)(2,1)S(1)}, u32[]{:S(2)}, u32[]{:S(2)}) %collective-permute-start.12) | collective-permute-done | bytes 524320 | tf_op jit(solution)/shard_map/ppermute | solution.py:30
  28.8 4.1 %scan_blocks.1 = (f32[4,128,128]{2,1,0:T(8,128)}, bf16[4,64,128]{2,1,0:T(8,128)(2,1)}) custom-call(bf16[128,256]{1,0:T(8,128)(2,1)} %query_ref.1, bf16[128,256]{1,0:T(8,128)(2,1)} %key_ref.1, bf16[128,256]{1,0:T(8,128)(2,1)} %value_ref.1, bf16[128,256]{1,0:T(8,128)(2,1)} %decay_ref.1, f32[128,256]{1,0:T(8,128)} %boost_ref.1, bf16[128,256]{1,0:T(8,128)(2,1)} %rate_ref.1), custom_call_target="tpu_custom_call" | custom-call | flops 4000000000 | bytes 1048576 | tf_op jit(solution)/shard_map/scan_blocks/pallas_call | solution.py:306
  33.0 1.4 collective-permute-done.other_ref.first_ref
  36.1 7.2 %collective-permute-start.3 = (bf16[2,64,128]{2,1,0:T(8,128)(2,1)S(1)}, bf16[2,64,128]{2,1,0:T(8,128)(2,1)S(1)}, u32[]{:S(2)}, u32[]{:S(2)}) collective-permute-start(bf16[2,64,128]{2,1,0:T(8,128)(2,1)S(1)} %get-tuple-element.25), channel_id=1, source_target_pairs={{0,24},{8,0},{16,8},{24,16},{32,56},{40,32},{48,40},{56,48},{64,88... | collective-permute-start | bytes 98312 | tf_op jit(solution)/shard_map/ppermute | solution.py:36
  43.3 1.6 collective-permute-done.3.refs_2_
  44.9 3.2 %collective-permute-done.2.refs_1_ = bf16[2,64,128]{2,1,0:T(8,128)(2,1)S(1)} collective-permute-done((bf16[2,64,128]{2,1,0:T(8,128)(2,1)S(1)}, bf16[2,64,128]{2,1,0:T(8,128)(2,1)S(1)}, u32[]{:S(2)}, u32[]{:S(2)}) %collective-permute-start.2) | collective-permute-done | bytes 32800 | tf_op jit(solution)/shard_map/ppermute | solution.py:36
  48.1 2.9 %collective-permute-done.1.refs_0_ = bf16[2,64,128]{2,1,0:T(8,128)(2,1)S(1)} collective-permute-done((bf16[2,64,128]{2,1,0:T(8,128)(2,1)S(1)}, bf16[2,64,128]{2,1,0:T(8,128)(2,1)S(1)}, u32[]{:S(2)}, u32[]{:S(2)}) %collective-permute-start.1) | collective-permute-done | bytes 32800 | tf_op jit(solution)/shard_map/ppermute | solution.py:36
  52.5 12.6 %collective-permute-start.6 = (bf16[2,64,128]{2,1,0:T(8,128)(2,1)S(1)}, bf16[2,64,128]{2,1,0:T(8,128)(2,1)S(1)}, u32[]{:S(2)}, u32[]{:S(2)}) collective-permute-start(bf16[2,64,128]{2,1,0:T(8,128)(2,1)S(1)} %get-tuple-element.27), channel_id=1, source_target_pairs={{0,32},{8,40},{16,48},{24,56},{32,64},{40,72},{48,80},{56,88},{64,... | collective-permute-start | bytes 98312 | tf_op jit(solution)/shard_map/ppermute | solution.py:41
  65.1 15.1 %collective-permute-start.5 = (bf16[2,64,128]{2,1,0:T(8,128)(2,1)S(1)}, bf16[2,64,128]{2,1,0:T(8,128)(2,1)S(1)}, u32[]{:S(2)}, u32[]{:S(2)}) collective-permute-start(bf16[2,64,128]{2,1,0:T(8,128)(2,1)S(1)} %get-tuple-element.27), channel_id=1, source_target_pairs={{0,64},{8,72},{16,80},{24,88},{32,96},{40,104},{48,112},{56,120},{... | collective-permute-start | bytes 98312 | tf_op jit(solution)/shard_map/ppermute | solution.py:41
  80.2 2.4 %collective-permute-start.4 = (bf16[2,64,128]{2,1,0:T(8,128)(2,1)S(1)}, bf16[2,64,128]{2,1,0:T(8,128)(2,1)S(1)}, u32[]{:S(2)}, u32[]{:S(2)}) collective-permute-start(bf16[2,64,128]{2,1,0:T(8,128)(2,1)S(1)} %get-tuple-element.27), channel_id=1, source_target_pairs={{0,96},{8,104},{16,112},{24,120},{1,97},{9,105},{17,113},{25,121},... | collective-permute-start | bytes 98312 | tf_op jit(solution)/shard_map/ppermute | solution.py:41
  82.6 1.6 collective-permute-done.4.refs_0_
  87.2 1.4 finish_heads.1
  89.7 2.2 collective-permute-start.9
  91.9 1.7 collective-permute-done.8.refs_0_
  93.6 1.3 collective-permute-start.10
  95.1 3.8 %collective-permute-done.10.refs_2_ = bf16[32,256]{1,0:T(8,128)(2,1)S(1)} collective-permute-done((bf16[32,256]{1,0:T(8,128)(2,1)S(1)}, bf16[32,256]{1,0:T(8,128)(2,1)S(1)}, u32[]{:S(2)}, u32[]{:S(2)}) %collective-permute-start.10) | collective-permute-done | bytes 16416 | tf_op jit(solution)/shard_map/ppermute | solution.py:30
  99.8 2.4 %project_rows.1 = (f32[32,2048]{1,0:T(8,128)S(1)}, bf16[128,2048]{1,0:T(8,128)(2,1)S(1)}, bf16[64,128]{1,0:T(8,128)(2,1)S(1)}) custom-call(s32[1]{0:T(128)} %bitcast.core_ref, bf16[32,256]{1,0:T(8,128)(2,1)S(1)} %get-tuple-element.28.own_ref, bf16[256,2048]{1,0:T(8,128)(2,1)S(1)} %copy-done, bf16[32,256]{1,0:T(8,128)(2,1)S(1)} %collective-permute-done.8.refs_0_, ...), custom_call_target="tpu_custom_call" | custom-call | flops 800000000 | bytes 5242880 | tf_op jit(solution)/shard_map/project_rows/pallas_call | solution.py:395
  104.2 43.9 %all_to_all.10 = bf16[32,8,1024]{2,1,0:T(8,128)(2,1)S(1)} all-to-all(bf16[32,8,1024]{2,1,0:T(8,128)(2,1)S(1)} %reshape.29), channel_id=1, replica_groups=mesh['grp'=2,'sp_0'=16,'sp_1'=2,'tp'=4] {'sp_0','sp_1'}, dimensions={0} | all-to-all | bytes 1048576 | tf_op jit(solution)/shard_map/all_to_all | solution.py:556
  148.3 1.5 collective-permute-start.19
  150.4 5.1 %first_rows.1 = (bf16[128,2048]{1,0:T(8,128)(2,1)S(1)}, bf16[2048,896]{1,0:T(8,128)(2,1)S(1)}, bf16[2048,896]{1,0:T(8,128)(2,1)S(1)}, bf16[896,2048]{1,0:T(8,128)(2,1)S(1)}) custom-call(bf16[128,2048]{1,0:T(8,128)(2,1)S(1)} %reshape.30.rows, bf16[2048,896]{1,0:T(8,128)(2,1)} %bitcast.11, bf16[2048,896]{1,0:T(8,128)(2,1)} %bitcast.12, bf16[896,2048]{1,0:T(8,128)(2,1)} %bitcast.13), custom_call_target="tpu_custom_call" | custom-call | flops 1409286144 | bytes 11010048 | tf_op jit(solution)/shard_map/first_rows/pallas_call | solution.py:467
  155.6 6.7 %collective-permute-done.19.refs_0_ = bf16[128,2048]{1,0:T(8,128)(2,1)S(1)} collective-permute-done((bf16[128,2048]{1,0:T(8,128)(2,1)S(1)}, bf16[128,2048]{1,0:T(8,128)(2,1)S(1)}, u32[]{:S(2)}, u32[]{:S(2)}) %collective-permute-start.19) | collective-permute-done | bytes 524320 | tf_op jit(solution)/shard_map/ppermute | solution.py:30
  162.3 2.7 %collective-permute-start.22 = (bf16[64,2048]{1,0:T(8,128)(2,1)S(1)}, bf16[64,2048]{1,0:T(8,128)(2,1)S(1)}, u32[]{:S(2)}, u32[]{:S(2)}) collective-permute-start(bf16[64,2048]{1,0:T(8,128)(2,1)S(1)} %slice.9), channel_id=1, source_target_pairs={{0,3},{1,0},{2,1},{3,2},{4,7},{5,4},{6,5},{7,6},{8,11},{9,8},{10,9... | collective-permute-start | bytes 786440 | tf_op jit(solution)/shard_map/ppermute | solution.py:30
  165.2 1.8 more_rows.3
  167.0 3.5 %collective-permute-start.18 = (bf16[128,2048]{1,0:T(8,128)(2,1)S(1)}, bf16[128,2048]{1,0:T(8,128)(2,1)S(1)}, u32[]{:S(2)}, u32[]{:S(2)}) collective-permute-start(bf16[128,2048]{1,0:T(8,128)(2,1)S(1)} %more_rows.3), channel_id=1, source_target_pairs={{0,3},{1,0},{2,1},{3,2},{4,7},{5,4},{6,5},{7,6},{8,11},{9,8},{10,9... | collective-permute-start | bytes 1572872 | tf_op jit(solution)/shard_map/ppermute | solution.py:30
  170.5 1.8 more_rows.4
  173.4 1.8 more_rows.5
  175.9 16.5 %collective-permute-done.18 = bf16[128,2048]{1,0:T(8,128)(2,1)S(1)} collective-permute-done((bf16[128,2048]{1,0:T(8,128)(2,1)S(1)}, bf16[128,2048]{1,0:T(8,128)(2,1)S(1)}, u32[]{:S(2)}, u32[]{:S(2)}) %collective-permute-start.18) | collective-permute-done | bytes 524320 | tf_op jit(solution)/shard_map/ppermute | solution.py:30
  192.4 4.7 %collective-permute-done.20 = bf16[128,2048]{1,0:T(8,128)(2,1)S(1)} collective-permute-done((bf16[128,2048]{1,0:T(8,128)(2,1)S(1)}, bf16[128,2048]{1,0:T(8,128)(2,1)S(1)}, u32[]{:S(2)}, u32[]{:S(2)}) %collective-permute-start.20) | collective-permute-done | bytes 524320 | tf_op jit(solution)/shard_map/ppermute | solution.py:30
  198.3 4.8 %all-to-all-start.1 = ((bf16[32,8,1024]{2,1,0:T(8,128)(2,1)}), bf16[32,8,1024]{2,1,0:T(8,128)(2,1)S(1)}, u32[]{:S(2)}, u32[]{:S(2)}) async-start(bf16[32,8,1024]{2,1,0:T(8,128)(2,1)} %reshape.31), calls=%async_computation.1 | async-start | bytes 1048576 | tf_op jit(solution)/shard_map/all_to_all | solution.py:571
  203.2 33.1 %all-to-all-done.1 = bf16[32,8,1024]{2,1,0:T(8,128)(2,1)S(1)} async-done(((bf16[32,8,1024]{2,1,0:T(8,128)(2,1)}), bf16[32,8,1024]{2,1,0:T(8,128)(2,1)S(1)}, u32[]{:S(2)}, u32[]{:S(2)}) %all-to-all-start.1) | async-done | bytes 524320 | tf_op jit(solution)/shard_map/all_to_all | solution.py:571
  (66 shorter events, 19.2 us)
Async XLA Ops:
  1.1 85.1 %copy-start.4 = (bf16[128,256]{1,0:T(8,128)(2,1)S(1)}, bf16[128,256]{1,0:T(8,128)(2,1)}, u32[]{:S(2)}) copy-start(bf16[128,256]{1,0:T(8,128)(2,1)} %gate_ref.1) | copy-start | bytes 196612
  1.1 85.1 %copy-start.6 = (f32[256]{0:T(256)S(1)}, f32[256]{0:T(256)}, u32[]{:S(2)}) copy-start(f32[256]{0:T(256)} %param.23) | copy-start | bytes 3076
  1.1 16.5 %collective-permute-start.13 = (bf16[256,1024]{1,0:T(8,128)(2,1)S(1)}, bf16[256,1024]{1,0:T(8,128)(2,1)S(1)}, u32[]{:S(2)}, u32[]{:S(2)}) collective-permute-start(bf16[256,1024]{1,0:T(8,128)(2,1)S(1)} %constant_dynamic-slice_fusion), channel_id=1, source_target_pairs={{0,2},{1,3},{2,0},{3,1},{4,6},{5,7},{6,4},{7,5},{8,10},{9,11},{10,... | collective-permute-start | bytes 1572872 | tf_op jit(solution)/shard_map/ppermute | solution.py:30
  4.5 23.7 %collective-permute-start.12 = (bf16[256,1024]{1,0:T(8,128)(2,1)S(1)}, bf16[256,1024]{1,0:T(8,128)(2,1)S(1)}, u32[]{:S(2)}, u32[]{:S(2)}) collective-permute-start(bf16[256,1024]{1,0:T(8,128)(2,1)S(1)} %constant_dynamic-slice_fusion), channel_id=1, source_target_pairs={{0,3},{1,0},{2,1},{3,2},{4,7},{5,4},{6,5},{7,6},{8,11},{9,8},{10,9... | collective-permute-start | bytes 1572872 | tf_op jit(solution)/shard_map/ppermute | solution.py:30
  5.5 22.7 %collective-permute-start.11 = (bf16[256,1024]{1,0:T(8,128)(2,1)S(1)}, bf16[256,1024]{1,0:T(8,128)(2,1)S(1)}, u32[]{:S(2)}, u32[]{:S(2)}) collective-permute-start(bf16[256,1024]{1,0:T(8,128)(2,1)S(1)} %constant_dynamic-slice_fusion), channel_id=1, source_target_pairs={{0,1},{1,2},{2,3},{3,0},{4,5},{5,6},{6,7},{7,4},{8,9},{9,10},{10,1... | collective-permute-start | bytes 1572872 | tf_op jit(solution)/shard_map/ppermute | solution.py:30
  17.6 81.3 %collective-permute-start.16 = (bf16[256,1024]{1,0:T(8,128)(2,1)S(1)}, bf16[256,1024]{1,0:T(8,128)(2,1)S(1)}, u32[]{:S(2)}, u32[]{:S(2)}) collective-permute-start(bf16[256,1024]{1,0:T(8,128)(2,1)S(1)} %collective-permute-done.13.refs_5_), channel_id=1, source_target_pairs={{0,4},{4,0},{1,5},{5,1},{2,6},{6,2},{3,7},{7,3},{8,12},{12,8},{9,1... | collective-permute-start | bytes 1572872 | tf_op jit(solution)/shard_map/ppermute | solution.py:30
  28.2 70.7 %collective-permute-start.15 = (bf16[256,1024]{1,0:T(8,128)(2,1)S(1)}, bf16[256,1024]{1,0:T(8,128)(2,1)}, u32[]{:S(2)}, u32[]{:S(2)}) collective-permute-start(bf16[256,1024]{1,0:T(8,128)(2,1)S(1)} %collective-permute-done.12.refs_4_), channel_id=1, source_target_pairs={{0,4},{4,0},{1,5},{5,1},{2,6},{6,2},{3,7},{7,3},{8,12},{12,8},{9,1... | collective-permute-start | bytes 1572872 | tf_op jit(solution)/shard_map/ppermute | solution.py:30
  28.2 70.7 %collective-permute-start.14 = (bf16[256,1024]{1,0:T(8,128)(2,1)S(1)}, bf16[256,1024]{1,0:T(8,128)(2,1)}, u32[]{:S(2)}, u32[]{:S(2)}) collective-permute-start(bf16[256,1024]{1,0:T(8,128)(2,1)S(1)} %collective-permute-done.11.refs_3_), channel_id=1, source_target_pairs={{0,4},{4,0},{1,5},{5,1},{2,6},{6,2},{3,7},{7,3},{8,12},{12,8},{9,1... | collective-permute-start | bytes 1572872 | tf_op jit(solution)/shard_map/ppermute | solution.py:30
  28.7 66.2 %copy-start.10 = (s32[32,2]{0,1:T(2,128)S(1)}, s32[32,2]{0,1:T(2,128)}, u32[]{:S(2)}) copy-start(s32[32,2]{0,1:T(2,128)} %param.27) | copy-start | bytes 772
  32.9 66.0 %copy-start = (bf16[256,2048]{1,0:T(8,128)(2,1)S(1)}, bf16[256,2048]{1,0:T(8,128)(2,1)}, u32[]{:S(2)}) copy-start(bf16[256,2048]{1,0:T(8,128)(2,1)} %weight_ref.2) | copy-start | bytes 3145732
  32.9 66.0 %copy-start.3 = (f32[2048]{0:T(1024)S(1)}, f32[2048]{0:T(1024)}, u32[]{:S(2)}) copy-start(f32[2048]{0:T(1024)} %param.26) | copy-start | bytes 24580
  32.9 1.6 collective-permute-start
  36.1 8.8 %collective-permute-start.3 = (bf16[2,64,128]{2,1,0:T(8,128)(2,1)S(1)}, bf16[2,64,128]{2,1,0:T(8,128)(2,1)S(1)}, u32[]{:S(2)}, u32[]{:S(2)}) collective-permute-start(bf16[2,64,128]{2,1,0:T(8,128)(2,1)S(1)} %get-tuple-element.25), channel_id=1, source_target_pairs={{0,24},{8,0},{16,8},{24,16},{32,56},{40,32},{48,40},{56,48},{64,88... | collective-permute-start | bytes 98312 | tf_op jit(solution)/shard_map/ppermute | solution.py:36
  43.3 4.8 %collective-permute-start.2 = (bf16[2,64,128]{2,1,0:T(8,128)(2,1)S(1)}, bf16[2,64,128]{2,1,0:T(8,128)(2,1)S(1)}, u32[]{:S(2)}, u32[]{:S(2)}) collective-permute-start(bf16[2,64,128]{2,1,0:T(8,128)(2,1)S(1)} %get-tuple-element.25), channel_id=1, source_target_pairs={{0,16},{8,24},{16,0},{24,8},{32,48},{40,56},{48,32},{56,40},{64,80... | collective-permute-start | bytes 98312 | tf_op jit(solution)/shard_map/ppermute | solution.py:36
  44.9 6.1 %collective-permute-start.1 = (bf16[2,64,128]{2,1,0:T(8,128)(2,1)S(1)}, bf16[2,64,128]{2,1,0:T(8,128)(2,1)S(1)}, u32[]{:S(2)}, u32[]{:S(2)}) collective-permute-start(bf16[2,64,128]{2,1,0:T(8,128)(2,1)S(1)} %get-tuple-element.25), channel_id=1, source_target_pairs={{0,8},{8,16},{16,24},{24,0},{32,40},{40,48},{48,56},{56,32},{64,72... | collective-permute-start | bytes 98312 | tf_op jit(solution)/shard_map/ppermute | solution.py:36
  52.5 27.7 %collective-permute-start.6 = (bf16[2,64,128]{2,1,0:T(8,128)(2,1)S(1)}, bf16[2,64,128]{2,1,0:T(8,128)(2,1)S(1)}, u32[]{:S(2)}, u32[]{:S(2)}) collective-permute-start(bf16[2,64,128]{2,1,0:T(8,128)(2,1)S(1)} %get-tuple-element.27), channel_id=1, source_target_pairs={{0,32},{8,40},{16,48},{24,56},{32,64},{40,72},{48,80},{56,88},{64,... | collective-permute-start | bytes 98312 | tf_op jit(solution)/shard_map/ppermute | solution.py:41
  65.1 17.6 %collective-permute-start.5 = (bf16[2,64,128]{2,1,0:T(8,128)(2,1)S(1)}, bf16[2,64,128]{2,1,0:T(8,128)(2,1)S(1)}, u32[]{:S(2)}, u32[]{:S(2)}) collective-permute-start(bf16[2,64,128]{2,1,0:T(8,128)(2,1)S(1)} %get-tuple-element.27), channel_id=1, source_target_pairs={{0,64},{8,72},{16,80},{24,88},{32,96},{40,104},{48,112},{56,120},{... | collective-permute-start | bytes 98312 | tf_op jit(solution)/shard_map/ppermute | solution.py:41
  80.2 4.0 %collective-permute-start.4 = (bf16[2,64,128]{2,1,0:T(8,128)(2,1)S(1)}, bf16[2,64,128]{2,1,0:T(8,128)(2,1)S(1)}, u32[]{:S(2)}, u32[]{:S(2)}) collective-permute-start(bf16[2,64,128]{2,1,0:T(8,128)(2,1)S(1)} %get-tuple-element.27), channel_id=1, source_target_pairs={{0,96},{8,104},{16,112},{24,120},{1,97},{9,105},{17,113},{25,121},... | collective-permute-start | bytes 98312 | tf_op jit(solution)/shard_map/ppermute | solution.py:41
  84.9 1.3 collective-permute-start.7
  86.2 1.0 copy-start.7
  88.6 5.1 %collective-permute-start.8 = (bf16[32,256]{1,0:T(8,128)(2,1)S(1)}, bf16[32,256]{1,0:T(8,128)(2,1)S(1)}, u32[]{:S(2)}, u32[]{:S(2)}) collective-permute-start(bf16[32,256]{1,0:T(8,128)(2,1)S(1)} %get-tuple-element.29), channel_id=1, source_target_pairs={{0,1},{1,2},{2,3},{3,0},{4,5},{5,6},{6,7},{7,4},{8,9},{9,10},{10,1... | collective-permute-start | bytes 49160 | tf_op jit(solution)/shard_map/ppermute | solution.py:30
  89.7 5.3 %collective-permute-start.9 = (bf16[32,256]{1,0:T(8,128)(2,1)S(1)}, bf16[32,256]{1,0:T(8,128)(2,1)S(1)}, u32[]{:S(2)}, u32[]{:S(2)}) collective-permute-start(bf16[32,256]{1,0:T(8,128)(2,1)S(1)} %get-tuple-element.30), channel_id=1, source_target_pairs={{0,3},{1,0},{2,1},{3,2},{4,7},{5,4},{6,5},{7,6},{8,11},{9,8},{10,9... | collective-permute-start | bytes 49160 | tf_op jit(solution)/shard_map/ppermute | solution.py:30
  93.6 5.2 %collective-permute-start.10 = (bf16[32,256]{1,0:T(8,128)(2,1)S(1)}, bf16[32,256]{1,0:T(8,128)(2,1)S(1)}, u32[]{:S(2)}, u32[]{:S(2)}) collective-permute-start(bf16[32,256]{1,0:T(8,128)(2,1)S(1)} %get-tuple-element.31), channel_id=1, source_target_pairs={{0,2},{1,3},{2,0},{3,1},{4,6},{5,7},{6,4},{7,5},{8,10},{9,11},{10,... | collective-permute-start | bytes 49160 | tf_op jit(solution)/shard_map/ppermute | solution.py:30
  148.3 13.9 %collective-permute-start.19 = (bf16[128,2048]{1,0:T(8,128)(2,1)S(1)}, bf16[128,2048]{1,0:T(8,128)(2,1)S(1)}, u32[]{:S(2)}, u32[]{:S(2)}) collective-permute-start(bf16[128,2048]{1,0:T(8,128)(2,1)S(1)} %reshape.30.rows), channel_id=1, source_target_pairs={{0,3},{1,0},{2,1},{3,2},{4,7},{5,4},{6,5},{7,6},{8,11},{9,8},{10,9... | collective-permute-start | bytes 1572872 | tf_op jit(solution)/shard_map/ppermute | solution.py:30
  149.8 15.2 %collective-permute-start.17 = (bf16[128,2048]{1,0:T(8,128)(2,1)S(1)}, bf16[128,2048]{1,0:T(8,128)(2,1)S(1)}, u32[]{:S(2)}, u32[]{:S(2)}) collective-permute-start(bf16[128,2048]{1,0:T(8,128)(2,1)S(1)} %reshape.30.rows), channel_id=1, source_target_pairs={{0,1},{1,2},{2,3},{3,0},{4,5},{5,6},{6,7},{7,4},{8,9},{9,10},{10,1... | collective-permute-start | bytes 1572872 | tf_op jit(solution)/shard_map/ppermute | solution.py:30
  162.3 10.2 %collective-permute-start.22 = (bf16[64,2048]{1,0:T(8,128)(2,1)S(1)}, bf16[64,2048]{1,0:T(8,128)(2,1)S(1)}, u32[]{:S(2)}, u32[]{:S(2)}) collective-permute-start(bf16[64,2048]{1,0:T(8,128)(2,1)S(1)} %slice.9), channel_id=1, source_target_pairs={{0,3},{1,0},{2,1},{3,2},{4,7},{5,4},{6,5},{7,6},{8,11},{9,8},{10,9... | collective-permute-start | bytes 786440 | tf_op jit(solution)/shard_map/ppermute | solution.py:30
  165.0 8.4 %collective-permute-start.21 = (bf16[64,2048]{1,0:T(8,128)(2,1)S(1)}, bf16[64,2048]{1,0:T(8,128)(2,1)S(1)}, u32[]{:S(2)}, u32[]{:S(2)}) collective-permute-start(bf16[64,2048]{1,0:T(8,128)(2,1)S(1)} %slice.8), channel_id=1, source_target_pairs={{0,1},{1,2},{2,3},{3,0},{4,5},{5,6},{6,7},{7,4},{8,9},{9,10},{10,1... | collective-permute-start | bytes 786440 | tf_op jit(solution)/shard_map/ppermute | solution.py:30
  167.0 25.4 %collective-permute-start.18 = (bf16[128,2048]{1,0:T(8,128)(2,1)S(1)}, bf16[128,2048]{1,0:T(8,128)(2,1)S(1)}, u32[]{:S(2)}, u32[]{:S(2)}) collective-permute-start(bf16[128,2048]{1,0:T(8,128)(2,1)S(1)} %more_rows.3), channel_id=1, source_target_pairs={{0,3},{1,0},{2,1},{3,2},{4,7},{5,4},{6,5},{7,6},{8,11},{9,8},{10,9... | collective-permute-start | bytes 1572872 | tf_op jit(solution)/shard_map/ppermute | solution.py:30
  172.3 24.7 %collective-permute-start.20 = (bf16[128,2048]{1,0:T(8,128)(2,1)S(1)}, bf16[128,2048]{1,0:T(8,128)(2,1)S(1)}, u32[]{:S(2)}, u32[]{:S(2)}) collective-permute-start(bf16[128,2048]{1,0:T(8,128)(2,1)S(1)} %more_rows.4), channel_id=1, source_target_pairs={{0,1},{1,2},{2,3},{3,0},{4,5},{5,6},{6,7},{7,4},{8,9},{9,10},{10,1... | collective-permute-start | bytes 1572872 | tf_op jit(solution)/shard_map/ppermute | solution.py:30
  175.2 27.9 %copy-start.11 = (f32[32,2]{0,1:T(2,128)S(1)}, f32[32,2]{0,1:T(2,128)}, u32[]{:S(2)}) copy-start(f32[32,2]{0,1:T(2,128)} %param.28) | copy-start | bytes 772
  175.3 21.8 %collective-permute-start.23 = (bf16[128,2048]{1,0:T(8,128)(2,1)S(1)}, bf16[128,2048]{1,0:T(8,128)(2,1)S(1)}, u32[]{:S(2)}, u32[]{:S(2)}) collective-permute-start(bf16[128,2048]{1,0:T(8,128)(2,1)S(1)} %more_rows.5), channel_id=1, source_target_pairs={{0,2},{1,3},{2,0},{3,1},{4,6},{5,7},{6,4},{7,5},{8,10},{9,11},{10,... | collective-permute-start | bytes 1572872 | tf_op jit(solution)/shard_map/ppermute | solution.py:30
  198.3 38.0 %all-to-all-start.1 = ((bf16[32,8,1024]{2,1,0:T(8,128)(2,1)}), bf16[32,8,1024]{2,1,0:T(8,128)(2,1)S(1)}, u32[]{:S(2)}, u32[]{:S(2)}) async-start(bf16[32,8,1024]{2,1,0:T(8,128)(2,1)} %reshape.31), calls=%async_computation.1 | async-start | bytes 1048576 | tf_op jit(solution)/shard_map/all_to_all | solution.py:571
  (5 other events, 4.0 us)

commit v3 on v2

--- a/solution.py
+++ b/solution.py
@@ -362,9 +362,9 @@
     )(place, outputs, first, mine, swapped, gate_logits, gain.reshape(1, -1))
 
 
-def project_kernel(count, capacity, core_ref, own_ref, weight_ref, *refs):
+def project_kernel(count, core_ref, own_ref, weight_ref, *refs):
     rows, mine, other = refs[:count], refs[count : 2 * count], refs[2 * count : 3 * count]
-    residual_ref, gain_ref, column_ref, line_ref, stream_ref, out_ref, onehot_ref = refs[3 * count :]
+    residual_ref, gain_ref, placed_ref, stream_ref, out_ref = refs[3 * count :]
     halves = []
     for side in (mine, other):
         halves.append(sum(plain_dot(r[...], w[...]) for r, w in zip(rows, side)))
@@ -376,56 +376,23 @@
     stream_ref[...] = stream
     scale = lax.rsqrt(jnp.mean(stream * stream, axis=1, keepdims=True) + 1e-06)
     normal = (stream * scale * gain_ref[...]).astype(jnp.bfloat16)
-    tokens, total = stream.shape[0], line_ref.shape[1]
-    expert = column_ref[...]
-    row = lax.broadcasted_iota(jnp.int32, (total, total), 0)
-    col = lax.broadcasted_iota(jnp.int32, (total, total), 1)
-    earlier = (expert == line_ref[...]) & (col < row)
-    rank = jnp.sum(earlier.astype(jnp.float32), axis=1, keepdims=True).astype(jnp.int32)
-    slot = lax.broadcasted_iota(jnp.int32, onehot_ref.shape, 1)
-    onehot = (expert * capacity + rank == slot).astype(jnp.float32)
-    onehot_ref[...] = onehot.astype(onehot_ref.dtype)
-    placed = sum(onehot[k : k + tokens] for k in range(0, total, tokens))
-    out_ref[...] = plain_dot(placed, normal, ((0,), (0,))).astype(out_ref.dtype)
-
-
-def projected(own, weight, rows, weights, residual, gain, routes, experts, capacity):
+    out_ref[...] = plain_dot(placed_ref[...], normal, ((0,), (0,))).astype(out_ref.dtype)
+
+
+def projected(own, weight, rows, weights, residual, gain, placed):
     count, width = len(rows), residual.shape[1]
-    flat = routes.T.reshape(-1)
-    return pl.pallas_call(
-        partial(project_kernel, count, capacity),
+    return pl.pallas_call(
+        partial(project_kernel, count),
         out_shape=(
             jax.ShapeDtypeStruct(residual.shape, jnp.float32),
-            jax.ShapeDtypeStruct((experts * capacity, width), jnp.bfloat16),
-            jax.ShapeDtypeStruct((routes.size, experts * capacity), jnp.bfloat16),
-        ),
-        in_specs=[pl.BlockSpec(memory_space=pltpu.SMEM), *in_vmem(3 * count + 6)],
-        out_specs=tuple(in_vmem(3)),
+            jax.ShapeDtypeStruct((placed.shape[1], width), jnp.bfloat16),
+        ),
+        in_specs=[pl.BlockSpec(memory_space=pltpu.SMEM), *in_vmem(3 * count + 5)],
+        out_specs=tuple(in_vmem(2)),
         cost_estimate=pl.CostEstimate(flops=800_000_000, bytes_accessed=5 << 20, transcendentals=0),
         compiler_params=pltpu.CompilerParams(vmem_limit_bytes=20 << 20),
         name="project_rows",
-    )(core_index(), own, weight, *rows, *weights[0], *weights[1], residual, gain.reshape(1, -1), flat.reshape(-1, 1), flat.reshape(1, -1))
-
-
-def combine_kernel(onehot_ref, weight_ref, stream_ref, home_ref, out_ref):
-    tokens = stream_ref.shape[0]
-    picked = plain_dot(onehot_ref[...], home_ref[...])
-    total = stream_ref[...]
-    for k in range(weight_ref.shape[1]):
-        total = total + picked[k * tokens : (k + 1) * tokens] * weight_ref[:, k : k + 1]
-    out_ref[...] = total.astype(out_ref.dtype)
-
-
-def combined(onehot, weight, stream, home):
-    return pl.pallas_call(
-        combine_kernel,
-        out_shape=jax.ShapeDtypeStruct(stream.shape, jnp.bfloat16),
-        in_specs=in_vmem(4),
-        out_specs=in_vmem(1)[0],
-        compiler_params=pltpu.CompilerParams(vmem_limit_bytes=12 << 20),
-        cost_estimate=pl.CostEstimate(flops=100_000_000, bytes_accessed=1 << 20, transcendentals=0),
-        name="combine_rows",
-    )(onehot, weight, stream, home)
+    )(core_index(), own, weight, *rows, *weights[0], *weights[1], residual, gain.reshape(1, -1), placed)
 
 
 def hidden_rows(rows, gate, up):
@@ -540,17 +507,19 @@
     sp_count = lax.axis_size(SP)
     tp_count = lax.axis_size("tp")
     capacity = max(2, 2 * TOK_DEV * TOP // (tp_count * sp_count))
-    width_model = residual.shape[1]
-    stream, outbound, onehot = projected(
-        own,
-        output_weight,
-        rows_here,
-        weights,
-        residual,
-        expert_norm_gain,
-        routes,
-        sp_count,
-        capacity,
+    local_count, width_model = residual.shape
+    flat_routes = routes.reshape(-1)
+    expert_ids = jnp.arange(sp_count, dtype=jnp.int32)
+    chosen = (flat_routes[:, None] == expert_ids[None, :]).astype(jnp.int32)
+    earlier = jnp.cumsum(chosen, axis=0) - chosen
+    rank = jnp.sum(earlier * chosen, axis=1)
+    place = flat_routes * capacity + rank
+    places = jnp.arange(sp_count * capacity, dtype=jnp.int32)
+    onehot = (place[:, None] == places[None, :]).astype(jnp.bfloat16)
+    placed = jnp.sum(onehot.reshape(local_count, TOP, sp_count * capacity), axis=1)
+    placed, onehot, routing_weight = lax.optimization_barrier((placed, onehot, routing_weight))
+    stream, outbound = projected(
+        own, output_weight, rows_here, weights, residual, expert_norm_gain, placed
     )
     going = outbound.reshape(sp_count, 2 * capacity, width_model // 2)
     arrived = lax.all_to_all(going, SP, split_axis=0, concat_axis=0, tiled=True)
@@ -570,7 +539,11 @@
     total = total.reshape(sp_count, 2 * capacity, width_model // 2)
     home = lax.all_to_all(total, SP, split_axis=0, concat_axis=0, tiled=True)
     home = home.reshape(-1, width_model)
-    return combined(onehot, routing_weight, stream, home)
+    picked = jnp.dot(onehot, home, preferred_element_type=jnp.float32)
+    routed = jnp.sum(
+        picked.reshape(local_count, TOP, width_model) * routing_weight[:, :, None], axis=1
+    )
+    return (stream + routed).astype(jnp.bfloat16)
 
 
 def solution(mesh):

time: 239 us -> 212 us (0.89)
  waiting for transfers between devices: 101 us -> 42.7 us
  blocking collectives: 43.9 us -> 81 us
  starting transfers between devices: 62.2 us -> 56.6 us
    all_to_all x0 -> x1, blocking collectives: none -> 37.1 us  [body(): home = lax.all_to_all(total, SP, split_axis=0, concat_axis=0, tiled=True)]
    all_to_all x1 -> x0, waiting for transfers between devices: 33.1 us -> none  [body(): home = lax.all_to_all(total, SP, split_axis=0, concat_axis=0, tiled=True)]
    ppermute x18, waiting for transfers between devices: 58.5 us -> 35.5 us  [shifted(): return lax.ppermute(x, axis, [(i, (i + step) % size) for i in range(size)])]
    all_to_all x1 -> x0, starting transfers between devices: 4.8 us -> none  [body(): home = lax.all_to_all(total, SP, split_axis=0, concat_axis=0, tiled=True)]
    unnamed x25 -> x29, local copies, waits for them, and re-layouts: 5.05 us -> 4.19 us
  transfers between devices with their start and end apart: 25 -> 24, of which waited for: 15 -> 10; matrix products, arithmetic and copies ran while one was open for 0% -> 1% of each run, Pallas kernels for 7% -> 6%
where the time goes in v3:
time: 212 us; the launch traced here: 211 us
  blocking collectives  81 us (38%)
  starting transfers between devices  56.6 us (27%)
  waiting for transfers between devices  42.7 us (20%)
  Pallas kernels  20.1 us (9%)
  local copies, waits for them, and re-layouts  7.76 us (4%)
  other arithmetic  2.18 us (1%)
    all_to_all x1, blocking collectives, body(): arrived = lax.all_to_all(going, SP, split_axis=0, concat_axis=0, tiled=True)  43.9 us
    all_to_all x1, blocking collectives, body(): home = lax.all_to_all(total, SP, split_axis=0, concat_axis=0, tiled=True)  37.1 us
    ppermute x18, waiting for transfers between devices, shifted(): return lax.ppermute(x, axis, [(i, (i + step) % size) for i in range(size)])  35.5 us
    ppermute x3, starting transfers between devices, across_quads(): lax.ppermute(x, axis, [(i, i + step * QUAD) for i in range(size - step *...  30.1 us
    ppermute x18, starting transfers between devices, shifted(): return lax.ppermute(x, axis, [(i, (i + step) % size) for i in range(size)])  19 us
    ppermute x3, starting transfers between devices, within_quads(): return lax.ppermute(x, axis, pairs)  7.45 us
    ppermute x3, waiting for transfers between devices, within_quads(): return lax.ppermute(x, axis, pairs)  7.12 us
    pallas_call x3, Pallas kernels, more_rows(): pl.pallas_call(partial(more_kernel, len(pieces)), out_shape=jax.ShapeDtyp...  5.43 us
  transfers between devices with their start and end apart: 24, of which 10 were waited for; matrix products, arithmetic and copies ran while one was open for 1% of the time, Pallas kernels for 6%

profile of v3, /device:TPU:40, one launch (start us, length us, event | category | flops | bytes accessed | tf_op | source)
XLA Modules:
  0.0 210.8 jit_solution(12221535371854448165)
XLA Ops:
  0.0 4.2 %scan_blocks.1 = (f32[4,128,128]{2,1,0:T(8,128)}, bf16[4,64,128]{2,1,0:T(8,128)(2,1)}) custom-call(bf16[128,256]{1,0:T(8,128)(2,1)} %query_ref.1, bf16[128,256]{1,0:T(8,128)(2,1)} %key_ref.1, bf16[128,256]{1,0:T(8,128)(2,1)} %value_ref.1, bf16[128,256]{1,0:T(8,128)(2,1)} %decay_ref.1, f32[128,256]{1,0:T(8,128)} %boost_ref.1, bf16[128,256]{1,0:T(8,128)(2,1)} %rate_ref.1), custom_call_target="tpu_custom_call" | custom-call | flops 4000000000 | bytes 1048576 | tf_op jit(solution)/shard_map/scan_blocks/pallas_call | solution.py:306
  5.2 3.3 %collective-permute-start.13 = (bf16[256,1024]{1,0:T(8,128)(2,1)}, bf16[256,1024]{1,0:T(8,128)(2,1)S(1)}, u32[]{:S(2)}, u32[]{:S(2)}) collective-permute-start(bf16[256,1024]{1,0:T(8,128)(2,1)} %constant_dynamic-slice_fusion), channel_id=1, source_target_pairs={{0,2},{1,3},{2,0},{3,1},{4,6},{5,7},{6,4},{7,5},{8,10},{9,11},{10,... | collective-permute-start | bytes 1572872 | tf_op jit(solution)/shard_map/ppermute | solution.py:30
  8.5 1.0 collective-permute-start.12
  9.5 1.0 collective-permute-start.11
  11.8 7.3 %collective-permute-start.3 = (bf16[2,64,128]{2,1,0:T(8,128)(2,1)S(1)}, bf16[2,64,128]{2,1,0:T(8,128)(2,1)S(1)}, u32[]{:S(2)}, u32[]{:S(2)}) collective-permute-start(bf16[2,64,128]{2,1,0:T(8,128)(2,1)S(1)} %get-tuple-element.27), channel_id=1, source_target_pairs={{0,24},{8,0},{16,8},{24,16},{32,56},{40,32},{48,40},{56,48},{64,88... | collective-permute-start | bytes 98312 | tf_op jit(solution)/shard_map/ppermute | solution.py:36
  19.4 1.3 collective-permute-done.3.refs_2_
  20.9 3.3 %collective-permute-done.2.refs_1_ = bf16[2,64,128]{2,1,0:T(8,128)(2,1)S(1)} collective-permute-done((bf16[2,64,128]{2,1,0:T(8,128)(2,1)S(1)}, bf16[2,64,128]{2,1,0:T(8,128)(2,1)S(1)}, u32[]{:S(2)}, u32[]{:S(2)}) %collective-permute-start.2) | collective-permute-done | bytes 32800 | tf_op jit(solution)/shard_map/ppermute | solution.py:36
  24.2 2.5 %collective-permute-done.1.refs_0_ = bf16[2,64,128]{2,1,0:T(8,128)(2,1)S(1)} collective-permute-done((bf16[2,64,128]{2,1,0:T(8,128)(2,1)S(1)}, bf16[2,64,128]{2,1,0:T(8,128)(2,1)S(1)}, u32[]{:S(2)}, u32[]{:S(2)}) %collective-permute-start.1) | collective-permute-done | bytes 32800 | tf_op jit(solution)/shard_map/ppermute | solution.py:36
  28.0 12.5 %collective-permute-start.6 = (bf16[2,64,128]{2,1,0:T(8,128)(2,1)S(1)}, bf16[2,64,128]{2,1,0:T(8,128)(2,1)S(1)}, u32[]{:S(2)}, u32[]{:S(2)}) collective-permute-start(bf16[2,64,128]{2,1,0:T(8,128)(2,1)S(1)} %get-tuple-element.29), channel_id=1, source_target_pairs={{0,32},{8,40},{16,48},{24,56},{32,64},{40,72},{48,80},{56,88},{64,... | collective-permute-start | bytes 98312 | tf_op jit(solution)/shard_map/ppermute | solution.py:41
  40.6 15.1 %collective-permute-start.5 = (bf16[2,64,128]{2,1,0:T(8,128)(2,1)S(1)}, bf16[2,64,128]{2,1,0:T(8,128)(2,1)S(1)}, u32[]{:S(2)}, u32[]{:S(2)}) collective-permute-start(bf16[2,64,128]{2,1,0:T(8,128)(2,1)S(1)} %get-tuple-element.29), channel_id=1, source_target_pairs={{0,64},{8,72},{16,80},{24,88},{32,96},{40,104},{48,112},{56,120},{... | collective-permute-start | bytes 98312 | tf_op jit(solution)/shard_map/ppermute | solution.py:41
  55.7 2.4 %collective-permute-start.4 = (bf16[2,64,128]{2,1,0:T(8,128)(2,1)S(1)}, bf16[2,64,128]{2,1,0:T(8,128)(2,1)S(1)}, u32[]{:S(2)}, u32[]{:S(2)}) collective-permute-start(bf16[2,64,128]{2,1,0:T(8,128)(2,1)S(1)} %get-tuple-element.29), channel_id=1, source_target_pairs={{0,96},{8,104},{16,112},{24,120},{1,97},{9,105},{17,113},{25,121},... | collective-permute-start | bytes 98312 | tf_op jit(solution)/shard_map/ppermute | solution.py:41
  62.6 0.9 copy-done.7
  63.5 1.4 finish_heads.1
  65.8 2.5 %collective-permute-start.9 = (bf16[32,256]{1,0:T(8,128)(2,1)S(1)}, bf16[32,256]{1,0:T(8,128)(2,1)S(1)}, u32[]{:S(2)}, u32[]{:S(2)}) collective-permute-start(bf16[32,256]{1,0:T(8,128)(2,1)S(1)} %get-tuple-element.32), channel_id=1, source_target_pairs={{0,3},{1,0},{2,1},{3,2},{4,7},{5,4},{6,5},{7,6},{8,11},{9,8},{10,9... | collective-permute-start | bytes 49160 | tf_op jit(solution)/shard_map/ppermute | solution.py:30
  68.3 1.7 collective-permute-done.8.refs_0_
  70.3 5.0 %collective-permute-done.10.refs_2_ = bf16[32,256]{1,0:T(8,128)(2,1)S(1)} collective-permute-done((bf16[32,256]{1,0:T(8,128)(2,1)S(1)}, bf16[32,256]{1,0:T(8,128)(2,1)S(1)}, u32[]{:S(2)}, u32[]{:S(2)}) %collective-permute-start.10) | collective-permute-done | bytes 16416 | tf_op jit(solution)/shard_map/ppermute | solution.py:30
  75.3 2.4 %project_rows.1 = (f32[32,2048]{1,0:T(8,128)S(1)}, bf16[128,2048]{1,0:T(8,128)(2,1)S(1)}) custom-call(s32[1]{0:T(128)} %bitcast.core_ref, bf16[32,256]{1,0:T(8,128)(2,1)S(1)} %get-tuple-element.30.own_ref, bf16[256,2048]{1,0:T(8,128)(2,1)S(1)} %copy-done, bf16[32,256]{1,0:T(8,128)(2,1)S(1)} %collective-permute-done.8.refs_0_, ...), custom_call_target="tpu_custom_call" | custom-call | flops 800000000 | bytes 5242880 | tf_op jit(solution)/shard_map/project_rows/pallas_call | solution.py:384
  78.5 1.2 reshape.52
  79.7 43.9 %all_to_all.10 = bf16[32,8,1024]{2,1,0:T(8,128)(2,1)S(1)} all-to-all(bf16[32,8,1024]{2,1,0:T(8,128)(2,1)S(1)} %reshape.52), channel_id=1, replica_groups=mesh['grp'=2,'sp_0'=16,'sp_1'=2,'tp'=4] {'sp_0','sp_1'}, dimensions={0} | all-to-all | bytes 1048576 | tf_op jit(solution)/shard_map/all_to_all | solution.py:525
  123.8 1.1 collective-permute-start.19
  124.9 1.0 collective-permute-start.17
  125.9 5.1 %first_rows.1 = (bf16[128,2048]{1,0:T(8,128)(2,1)S(1)}, bf16[2048,896]{1,0:T(8,128)(2,1)S(1)}, bf16[2048,896]{1,0:T(8,128)(2,1)S(1)}, bf16[896,2048]{1,0:T(8,128)(2,1)S(1)}) custom-call(bf16[128,2048]{1,0:T(8,128)(2,1)S(1)} %reshape.53.rows, bf16[2048,896]{1,0:T(8,128)(2,1)} %bitcast.12, bf16[2048,896]{1,0:T(8,128)(2,1)} %bitcast.13, bf16[896,2048]{1,0:T(8,128)(2,1)} %bitcast.14), custom_call_target="tpu_custom_call" | custom-call | flops 1409286144 | bytes 11010048 | tf_op jit(solution)/shard_map/first_rows/pallas_call | solution.py:434
  131.0 6.7 %collective-permute-done.19.refs_0_ = bf16[128,2048]{1,0:T(8,128)(2,1)S(1)} collective-permute-done((bf16[128,2048]{1,0:T(8,128)(2,1)S(1)}, bf16[128,2048]{1,0:T(8,128)(2,1)S(1)}, u32[]{:S(2)}, u32[]{:S(2)}) %collective-permute-start.19) | collective-permute-done | bytes 524320 | tf_op jit(solution)/shard_map/ppermute | solution.py:30
  137.7 2.3 %collective-permute-start.22 = (bf16[64,2048]{1,0:T(8,128)(2,1)S(1)}, bf16[64,2048]{1,0:T(8,128)(2,1)S(1)}, u32[]{:S(2)}, u32[]{:S(2)}) collective-permute-start(bf16[64,2048]{1,0:T(8,128)(2,1)S(1)} %slice.9), channel_id=1, source_target_pairs={{0,3},{1,0},{2,1},{3,2},{4,7},{5,4},{6,5},{7,6},{8,11},{9,8},{10,9... | collective-permute-start | bytes 786440 | tf_op jit(solution)/shard_map/ppermute | solution.py:30
  140.2 1.8 more_rows.3
  142.0 3.5 %collective-permute-start.18 = (bf16[128,2048]{1,0:T(8,128)(2,1)S(1)}, bf16[128,2048]{1,0:T(8,128)(2,1)S(1)}, u32[]{:S(2)}, u32[]{:S(2)}) collective-permute-start(bf16[128,2048]{1,0:T(8,128)(2,1)S(1)} %more_rows.3), channel_id=1, source_target_pairs={{0,3},{1,0},{2,1},{3,2},{4,7},{5,4},{6,5},{7,6},{8,11},{9,8},{10,9... | collective-permute-start | bytes 1572872 | tf_op jit(solution)/shard_map/ppermute | solution.py:30
  145.6 1.8 more_rows.4
  147.5 0.9 collective-permute-done.21.refs_0_
  148.5 1.8 more_rows.5
  151.0 16.5 %collective-permute-done.18 = bf16[128,2048]{1,0:T(8,128)(2,1)S(1)} collective-permute-done((bf16[128,2048]{1,0:T(8,128)(2,1)S(1)}, bf16[128,2048]{1,0:T(8,128)(2,1)S(1)}, u32[]{:S(2)}, u32[]{:S(2)}) %collective-permute-start.18) | collective-permute-done | bytes 524320 | tf_op jit(solution)/shard_map/ppermute | solution.py:30
  167.4 4.7 %collective-permute-done.20 = bf16[128,2048]{1,0:T(8,128)(2,1)S(1)} collective-permute-done((bf16[128,2048]{1,0:T(8,128)(2,1)S(1)}, bf16[128,2048]{1,0:T(8,128)(2,1)S(1)}, u32[]{:S(2)}, u32[]{:S(2)}) %collective-permute-start.20) | collective-permute-done | bytes 524320 | tf_op jit(solution)/shard_map/ppermute | solution.py:30
  172.6 37.1 %all_to_all.11 = bf16[32,8,1024]{2,1,0:T(8,128)(2,1)S(1)} all-to-all(bf16[32,8,1024]{2,1,0:T(8,128)(2,1)S(1)} %reshape.54), channel_id=1, replica_groups=mesh['grp'=2,'sp_0'=16,'sp_1'=2,'tp'=4] {'sp_0','sp_1'}, dimensions={0} | all-to-all | bytes 1048576 | tf_op jit(solution)/shard_map/all_to_all | solution.py:540
  (78 shorter events, 13.0 us)
Async XLA Ops:
  0.0 10.6 %copy-start.11 = (s32[32,2]{0,1:T(2,128)S(1)}, s32[32,2]{0,1:T(2,128)}, u32[]{:S(2)}) copy-start(s32[32,2]{0,1:T(2,128)} %param.27) | copy-start | bytes 772
  0.0 62.5 %copy-start.6 = (f32[256]{0:T(256)S(1)}, f32[256]{0:T(256)}, u32[]{:S(2)}) copy-start(f32[256]{0:T(256)} %param.23) | copy-start | bytes 3076
  0.0 62.5 %copy-start.4 = (bf16[128,256]{1,0:T(8,128)(2,1)S(1)}, bf16[128,256]{1,0:T(8,128)(2,1)}, u32[]{:S(2)}) copy-start(bf16[128,256]{1,0:T(8,128)(2,1)} %gate_ref.1) | copy-start | bytes 196612
  4.2 71.0 %copy-start.2 = (bf16[32,2048]{1,0:T(8,128)(2,1)S(1)}, bf16[32,2048]{1,0:T(8,128)(2,1)}, u32[]{:S(2)}) copy-start(bf16[32,2048]{1,0:T(8,128)(2,1)} %refs_9_.1) | copy-start | bytes 393220
  4.2 71.0 %copy-start.3 = (f32[2048]{0:T(1024)S(1)}, f32[2048]{0:T(1024)}, u32[]{:S(2)}) copy-start(f32[2048]{0:T(1024)} %param.26) | copy-start | bytes 24580
  4.2 6.5 %collective-permute-start = (bf16[4,64,128]{2,1,0:T(8,128)(2,1)}, bf16[4,64,128]{2,1,0:T(8,128)(2,1)S(1)}, u32[]{:S(2)}, u32[]{:S(2)}) collective-permute-start(bf16[4,64,128]{2,1,0:T(8,128)(2,1)} %get-tuple-element.25.own_ref), channel_id=1, source_target_pairs={{0,4},{4,0},{1,5},{5,1},{2,6},{6,2},{3,7},{7,3},{8,12},{12,8},{9,1... | collective-permute-start | bytes 196616 | tf_op jit(solution)/shard_map/ppermute | solution.py:30
  5.2 52.9 %collective-permute-start.13 = (bf16[256,1024]{1,0:T(8,128)(2,1)}, bf16[256,1024]{1,0:T(8,128)(2,1)S(1)}, u32[]{:S(2)}, u32[]{:S(2)}) collective-permute-start(bf16[256,1024]{1,0:T(8,128)(2,1)} %constant_dynamic-slice_fusion), channel_id=1, source_target_pairs={{0,2},{1,3},{2,0},{3,1},{4,6},{5,7},{6,4},{7,5},{8,10},{9,11},{10,... | collective-permute-start | bytes 1572872 | tf_op jit(solution)/shard_map/ppermute | solution.py:30
  8.5 49.7 %collective-permute-start.12 = (bf16[256,1024]{1,0:T(8,128)(2,1)}, bf16[256,1024]{1,0:T(8,128)(2,1)S(1)}, u32[]{:S(2)}, u32[]{:S(2)}) collective-permute-start(bf16[256,1024]{1,0:T(8,128)(2,1)} %constant_dynamic-slice_fusion), channel_id=1, source_target_pairs={{0,3},{1,0},{2,1},{3,2},{4,7},{5,4},{6,5},{7,6},{8,11},{9,8},{10,9... | collective-permute-start | bytes 1572872 | tf_op jit(solution)/shard_map/ppermute | solution.py:30
  9.5 49.2 %collective-permute-start.11 = (bf16[256,1024]{1,0:T(8,128)(2,1)}, bf16[256,1024]{1,0:T(8,128)(2,1)S(1)}, u32[]{:S(2)}, u32[]{:S(2)}) collective-permute-start(bf16[256,1024]{1,0:T(8,128)(2,1)} %constant_dynamic-slice_fusion), channel_id=1, source_target_pairs={{0,1},{1,2},{2,3},{3,0},{4,5},{5,6},{6,7},{7,4},{8,9},{9,10},{10,1... | collective-permute-start | bytes 1572872 | tf_op jit(solution)/shard_map/ppermute | solution.py:30
  11.8 8.9 %collective-permute-start.3 = (bf16[2,64,128]{2,1,0:T(8,128)(2,1)S(1)}, bf16[2,64,128]{2,1,0:T(8,128)(2,1)S(1)}, u32[]{:S(2)}, u32[]{:S(2)}) collective-permute-start(bf16[2,64,128]{2,1,0:T(8,128)(2,1)S(1)} %get-tuple-element.27), channel_id=1, source_target_pairs={{0,24},{8,0},{16,8},{24,16},{32,56},{40,32},{48,40},{56,48},{64,88... | collective-permute-start | bytes 98312 | tf_op jit(solution)/shard_map/ppermute | solution.py:36
  19.3 4.9 %collective-permute-start.2 = (bf16[2,64,128]{2,1,0:T(8,128)(2,1)S(1)}, bf16[2,64,128]{2,1,0:T(8,128)(2,1)S(1)}, u32[]{:S(2)}, u32[]{:S(2)}) collective-permute-start(bf16[2,64,128]{2,1,0:T(8,128)(2,1)S(1)} %get-tuple-element.27), channel_id=1, source_target_pairs={{0,16},{8,24},{16,0},{24,8},{32,48},{40,56},{48,32},{56,40},{64,80... | collective-permute-start | bytes 98312 | tf_op jit(solution)/shard_map/ppermute | solution.py:36
  20.7 6.0 %collective-permute-start.1 = (bf16[2,64,128]{2,1,0:T(8,128)(2,1)S(1)}, bf16[2,64,128]{2,1,0:T(8,128)(2,1)S(1)}, u32[]{:S(2)}, u32[]{:S(2)}) collective-permute-start(bf16[2,64,128]{2,1,0:T(8,128)(2,1)S(1)} %get-tuple-element.27), channel_id=1, source_target_pairs={{0,8},{8,16},{16,24},{24,0},{32,40},{40,48},{48,56},{56,32},{64,72... | collective-permute-start | bytes 98312 | tf_op jit(solution)/shard_map/ppermute | solution.py:36
  20.9 37.2 %copy-start.12 = (s32[64]{0:T(128)}, s32[64]{0:T(128)S(1)}, u32[]{:S(2)}) copy-start(s32[64]{0:T(128)S(1)} %select_reduce_fusion) | copy-start | bytes 772
  28.0 27.7 %collective-permute-start.6 = (bf16[2,64,128]{2,1,0:T(8,128)(2,1)S(1)}, bf16[2,64,128]{2,1,0:T(8,128)(2,1)S(1)}, u32[]{:S(2)}, u32[]{:S(2)}) collective-permute-start(bf16[2,64,128]{2,1,0:T(8,128)(2,1)S(1)} %get-tuple-element.29), channel_id=1, source_target_pairs={{0,32},{8,40},{16,48},{24,56},{32,64},{40,72},{48,80},{56,88},{64,... | collective-permute-start | bytes 98312 | tf_op jit(solution)/shard_map/ppermute | solution.py:41
  40.6 19.0 %collective-permute-start.5 = (bf16[2,64,128]{2,1,0:T(8,128)(2,1)S(1)}, bf16[2,64,128]{2,1,0:T(8,128)(2,1)S(1)}, u32[]{:S(2)}, u32[]{:S(2)}) collective-permute-start(bf16[2,64,128]{2,1,0:T(8,128)(2,1)S(1)} %get-tuple-element.29), channel_id=1, source_target_pairs={{0,64},{8,72},{16,80},{24,88},{32,96},{40,104},{48,112},{56,120},{... | collective-permute-start | bytes 98312 | tf_op jit(solution)/shard_map/ppermute | solution.py:41
  55.7 4.0 %collective-permute-start.4 = (bf16[2,64,128]{2,1,0:T(8,128)(2,1)S(1)}, bf16[2,64,128]{2,1,0:T(8,128)(2,1)S(1)}, u32[]{:S(2)}, u32[]{:S(2)}) collective-permute-start(bf16[2,64,128]{2,1,0:T(8,128)(2,1)S(1)} %get-tuple-element.29), channel_id=1, source_target_pairs={{0,96},{8,104},{16,112},{24,120},{1,97},{9,105},{17,113},{25,121},... | collective-permute-start | bytes 98312 | tf_op jit(solution)/shard_map/ppermute | solution.py:41
  58.1 17.1 %collective-permute-start.16 = (bf16[256,1024]{1,0:T(8,128)(2,1)S(1)}, bf16[256,1024]{1,0:T(8,128)(2,1)S(1)}, u32[]{:S(2)}, u32[]{:S(2)}) collective-permute-start(bf16[256,1024]{1,0:T(8,128)(2,1)S(1)} %collective-permute-done.13.refs_5_), channel_id=1, source_target_pairs={{0,4},{4,0},{1,5},{5,1},{2,6},{6,2},{3,7},{7,3},{8,12},{12,8},{9,1... | collective-permute-start | bytes 1572872 | tf_op jit(solution)/shard_map/ppermute | solution.py:30
  58.3 17.0 %collective-permute-start.15 = (bf16[256,1024]{1,0:T(8,128)(2,1)S(1)}, bf16[256,1024]{1,0:T(8,128)(2,1)}, u32[]{:S(2)}, u32[]{:S(2)}) collective-permute-start(bf16[256,1024]{1,0:T(8,128)(2,1)S(1)} %collective-permute-done.12.refs_4_), channel_id=1, source_target_pairs={{0,4},{4,0},{1,5},{5,1},{2,6},{6,2},{3,7},{7,3},{8,12},{12,8},{9,1... | collective-permute-start | bytes 1572872 | tf_op jit(solution)/shard_map/ppermute | solution.py:30
  58.8 16.5 %collective-permute-start.14 = (bf16[256,1024]{1,0:T(8,128)(2,1)S(1)}, bf16[256,1024]{1,0:T(8,128)(2,1)}, u32[]{:S(2)}, u32[]{:S(2)}) collective-permute-start(bf16[256,1024]{1,0:T(8,128)(2,1)S(1)} %collective-permute-done.11.refs_3_), channel_id=1, source_target_pairs={{0,4},{4,0},{1,5},{5,1},{2,6},{6,2},{3,7},{7,3},{8,12},{12,8},{9,1... | collective-permute-start | bytes 1572872 | tf_op jit(solution)/shard_map/ppermute | solution.py:30
  61.2 1.3 collective-permute-start.7
  64.9 5.1 %collective-permute-start.8 = (bf16[32,256]{1,0:T(8,128)(2,1)S(1)}, bf16[32,256]{1,0:T(8,128)(2,1)S(1)}, u32[]{:S(2)}, u32[]{:S(2)}) collective-permute-start(bf16[32,256]{1,0:T(8,128)(2,1)S(1)} %get-tuple-element.31), channel_id=1, source_target_pairs={{0,1},{1,2},{2,3},{3,0},{4,5},{5,6},{6,7},{7,4},{8,9},{9,10},{10,1... | collective-permute-start | bytes 49160 | tf_op jit(solution)/shard_map/ppermute | solution.py:30
  65.8 4.5 %collective-permute-start.9 = (bf16[32,256]{1,0:T(8,128)(2,1)S(1)}, bf16[32,256]{1,0:T(8,128)(2,1)S(1)}, u32[]{:S(2)}, u32[]{:S(2)}) collective-permute-start(bf16[32,256]{1,0:T(8,128)(2,1)S(1)} %get-tuple-element.32), channel_id=1, source_target_pairs={{0,3},{1,0},{2,1},{3,2},{4,7},{5,4},{6,5},{7,6},{8,11},{9,8},{10,9... | collective-permute-start | bytes 49160 | tf_op jit(solution)/shard_map/ppermute | solution.py:30
  70.0 5.2 %collective-permute-start.10 = (bf16[32,256]{1,0:T(8,128)(2,1)S(1)}, bf16[32,256]{1,0:T(8,128)(2,1)S(1)}, u32[]{:S(2)}, u32[]{:S(2)}) collective-permute-start(bf16[32,256]{1,0:T(8,128)(2,1)S(1)} %get-tuple-element.33), channel_id=1, source_target_pairs={{0,2},{1,3},{2,0},{3,1},{4,6},{5,7},{6,4},{7,5},{8,10},{9,11},{10,... | collective-permute-start | bytes 49160 | tf_op jit(solution)/shard_map/ppermute | solution.py:30
  123.8 13.9 %collective-permute-start.19 = (bf16[128,2048]{1,0:T(8,128)(2,1)S(1)}, bf16[128,2048]{1,0:T(8,128)(2,1)S(1)}, u32[]{:S(2)}, u32[]{:S(2)}) collective-permute-start(bf16[128,2048]{1,0:T(8,128)(2,1)S(1)} %reshape.53.rows), channel_id=1, source_target_pairs={{0,3},{1,0},{2,1},{3,2},{4,7},{5,4},{6,5},{7,6},{8,11},{9,8},{10,9... | collective-permute-start | bytes 1572872 | tf_op jit(solution)/shard_map/ppermute | solution.py:30
  124.9 15.2 %collective-permute-start.17 = (bf16[128,2048]{1,0:T(8,128)(2,1)S(1)}, bf16[128,2048]{1,0:T(8,128)(2,1)S(1)}, u32[]{:S(2)}, u32[]{:S(2)}) collective-permute-start(bf16[128,2048]{1,0:T(8,128)(2,1)S(1)} %reshape.53.rows), channel_id=1, source_target_pairs={{0,1},{1,2},{2,3},{3,0},{4,5},{5,6},{6,7},{7,4},{8,9},{9,10},{10,1... | collective-permute-start | bytes 1572872 | tf_op jit(solution)/shard_map/ppermute | solution.py:30
  137.7 9.8 %collective-permute-start.22 = (bf16[64,2048]{1,0:T(8,128)(2,1)S(1)}, bf16[64,2048]{1,0:T(8,128)(2,1)S(1)}, u32[]{:S(2)}, u32[]{:S(2)}) collective-permute-start(bf16[64,2048]{1,0:T(8,128)(2,1)S(1)} %slice.9), channel_id=1, source_target_pairs={{0,3},{1,0},{2,1},{3,2},{4,7},{5,4},{6,5},{7,6},{8,11},{9,8},{10,9... | collective-permute-start | bytes 786440 | tf_op jit(solution)/shard_map/ppermute | solution.py:30
  140.1 8.4 %collective-permute-start.21 = (bf16[64,2048]{1,0:T(8,128)(2,1)S(1)}, bf16[64,2048]{1,0:T(8,128)(2,1)S(1)}, u32[]{:S(2)}, u32[]{:S(2)}) collective-permute-start(bf16[64,2048]{1,0:T(8,128)(2,1)S(1)} %slice.8), channel_id=1, source_target_pairs={{0,1},{1,2},{2,3},{3,0},{4,5},{5,6},{6,7},{7,4},{8,9},{9,10},{10,1... | collective-permute-start | bytes 786440 | tf_op jit(solution)/shard_map/ppermute | solution.py:30
  142.0 25.4 %collective-permute-start.18 = (bf16[128,2048]{1,0:T(8,128)(2,1)S(1)}, bf16[128,2048]{1,0:T(8,128)(2,1)S(1)}, u32[]{:S(2)}, u32[]{:S(2)}) collective-permute-start(bf16[128,2048]{1,0:T(8,128)(2,1)S(1)} %more_rows.3), channel_id=1, source_target_pairs={{0,3},{1,0},{2,1},{3,2},{4,7},{5,4},{6,5},{7,6},{8,11},{9,8},{10,9... | collective-permute-start | bytes 1572872 | tf_op jit(solution)/shard_map/ppermute | solution.py:30
  147.4 24.7 %collective-permute-start.20 = (bf16[128,2048]{1,0:T(8,128)(2,1)S(1)}, bf16[128,2048]{1,0:T(8,128)(2,1)S(1)}, u32[]{:S(2)}, u32[]{:S(2)}) collective-permute-start(bf16[128,2048]{1,0:T(8,128)(2,1)S(1)} %more_rows.4), channel_id=1, source_target_pairs={{0,1},{1,2},{2,3},{3,0},{4,5},{5,6},{6,7},{7,4},{8,9},{9,10},{10,1... | collective-permute-start | bytes 1572872 | tf_op jit(solution)/shard_map/ppermute | solution.py:30
  150.3 59.6 %copy-start.10 = (bf16[64,128]{1,0:T(8,128)(2,1)S(1)}, bf16[64,128]{1,0:T(8,128)(2,1)}, u32[]{:S(2)}) copy-start(bf16[64,128]{1,0:T(8,128)(2,1)} %fusion.3) | copy-start | bytes 49156
  150.3 59.6 %copy-start.13 = (f32[32,2]{0,1:T(2,128)S(1)}, f32[32,2]{0,1:T(2,128)}, u32[]{:S(2)}) copy-start(f32[32,2]{0,1:T(2,128)} %param.28) | copy-start | bytes 772
  150.3 21.8 %collective-permute-start.23 = (bf16[128,2048]{1,0:T(8,128)(2,1)S(1)}, bf16[128,2048]{1,0:T(8,128)(2,1)S(1)}, u32[]{:S(2)}, u32[]{:S(2)}) collective-permute-start(bf16[128,2048]{1,0:T(8,128)(2,1)S(1)} %more_rows.5), channel_id=1, source_target_pairs={{0,2},{1,3},{2,0},{3,1},{4,6},{5,7},{6,4},{7,5},{8,10},{9,11},{10,... | collective-permute-start | bytes 1572872 | tf_op jit(solution)/shard_map/ppermute | solution.py:30
  (6 other events, 8.5 us)
